TPU v7x, 512 devices: a 8x2x16 block of a 8x8x16 slice. The times are simulated.
512 devices in a mesh: grp: 2 (over y), dp: 8 (over x), kv: 16 (over z), tp: 2 (over core).
Axes of the slice: x: 8, y: 2, z: 16, core: 2. Of those that a mesh axis runs over, the one named last changes fastest.
The devices are a block of a 8x8x16 slice.
Arguments:
- tokens: bfloat16 [2048, 2048], P(('grp', 'dp'), ('kv', 'tp')), parts along dimension 0, may hold values from -6 to 6
- norm_gain: float32 [2048], P('kv'), may hold values from 0.1 to 1.9
- w_query: bfloat16 [2048, 512], P('kv', 'tp'), may hold values from -0.125 to 0.125
- w_key: bfloat16 [2048, 512], P('kv', 'tp'), may hold values from -0.125 to 0.125
- w_value: bfloat16 [2048, 1024], P('kv', 'tp'), may hold values from -0.125 to 0.125
- w_outgate: bfloat16 [2048, 1024], P('kv', 'tp'), may hold values from -0.125 to 0.125
- w_ingate: bfloat16 [2048, 8], P('kv'), may hold values from -0.125 to 0.125
- w_forget: bfloat16 [2048, 8], P('kv'), may hold values from -0.125 to 0.125
- in_bias: float32 [8], replicated, may hold values from -1.5 to 0.5
- forget_bias: float32 [8], replicated, may hold values from -1 to 4
- memory: float32 [2048, 8, 64, 128], P(('grp', 'dp', 'kv'), 'tp'), parts along dimension 0, may hold values from -4 to 4
- normalizer: float32 [2048, 512], P(('grp', 'dp', 'kv'), 'tp'), parts along dimension 0, may hold values from -4 to 4
- stabilizer: float32 [2048, 8], P(('grp', 'dp', 'kv'), 'tp'), parts along dimension 0, may hold values from -1 to 1
- w_out: bfloat16 [1024, 2048], P('tp', 'kv'), may hold values from -0.1875 to 0.1875
- mlp_gain: float32 [2048], replicated, may hold values from 0.1 to 1.9
- w_up: bfloat16 [2048, 8192], P(None, ('kv', 'tp')), may hold values from -0.125 to 0.125
- w_down: bfloat16 [8192, 2048], P(('kv', 'tp')), may hold values from -0.125 to 0.125
Outputs:
- mixed_out: bfloat16 [2048, 2048], P(('grp', 'dp'), ('kv', 'tp')), parts along dimension 0
- memory_new: float32 [2048, 8, 64, 128], P(('grp', 'dp', 'kv'), 'tp'), parts along dimension 0
- normalizer_new: float32 [2048, 512], P(('grp', 'dp', 'kv'), 'tp'), parts along dimension 0
- stabilizer_new: float32 [2048, 8], P(('grp', 'dp', 'kv'), 'tp'), parts along dimension 0
There are 2 independent parts, one for each index of `grp`. A program takes and returns all parts, laid end to end along the dimension named above; an argument that names none is the same for every part. Nothing has to cross between parts.
All inputs are finite; a program needn't handle non-finite values.
Results may differ from a plain program's by a relative error of at most 0.03.
Values may be sent and summed in bfloat16 or wider, within the bound.
A program may use at most 64 MiB of HBM per device.

v0:
```python
import jax
import jax.numpy as jnp
from jax import lax
from jax.sharding import PartitionSpec as P

EPSILON = 1e-06


def joined_along(tiles, dim):
    lengths = list(tiles.shape[1:])
    lengths[dim] *= tiles.shape[0]
    return jnp.moveaxis(tiles, 0, dim).reshape(lengths)


def copy_for_each(x, axis):
    copies = jnp.broadcast_to(x, (lax.axis_size(axis), *x.shape))
    return lax.all_to_all(copies, axis, split_axis=0, concat_axis=0, tiled=True)


def gather_directly(x, axis, dim):
    return joined_along(copy_for_each(x, axis), dim)


def cut_along(x, dim, peers):
    before, after = (x.shape[:dim], x.shape[dim + 1 :])
    return jnp.moveaxis(x.reshape(*before, peers, -1, *after), dim, 0)


def sum_at_owner(x, axis, dim):
    tiles = cut_along(x, dim, lax.axis_size(axis))
    arrived = lax.all_to_all(tiles, axis, split_axis=0, concat_axis=0, tiled=True)
    return arrived.astype(jnp.float32).sum(axis=0)


def in_one_piece(arrays, axis, dim, along):
    both = jnp.concatenate(arrays, axis=along)
    out, at, gathered = (sum_at_owner(both, axis, dim), 0, [])
    for a in arrays:
        gathered.append(lax.slice_in_dim(out, at, at + a.shape[along], axis=along))
        at += a.shape[along]
    return tuple(gathered)


def gather_in_order(x, axes, turns):
    tiles = x[None]
    for k in turns:
        tiles = lax.all_gather(tiles, axes[k], axis=0, tiled=True)
    block = [lax.axis_size(axes[k]) for k in reversed(turns)]
    tiles = tiles.reshape(*block, *x.shape)
    turned = sorted(range(len(turns)), key=lambda place: turns[len(turns) - 1 - place])
    return tiles.transpose(*turned, *range(len(turns), tiles.ndim)).reshape(-1, *x.shape)


def gathered_by_axis(x, axes, turns, dim):
    return joined_along(gather_in_order(x, axes, turns), dim)


def channel_mix(rows_in, mlp_gain, w_up, w_down):
    rows_f = rows_in.astype(jnp.float32)
    rscale_mid = lax.rsqrt(jnp.mean(rows_f * rows_f, axis=1, keepdims=True) + EPSILON)
    normed = (rows_f * rscale_mid * mlp_gain).astype(jnp.bfloat16)
    upward = jnp.dot(normed, w_up, preferred_element_type=jnp.float32)
    squared = jnp.square(jax.nn.relu(upward)).astype(jnp.bfloat16)
    return jnp.dot(squared, w_down, preferred_element_type=jnp.float32).astype(jnp.bfloat16)


def shards(
    tokens,
    norm_gain,
    w_query,
    w_key,
    w_value,
    w_outgate,
    w_ingate,
    w_forget,
    in_bias,
    forget_bias,
    memory,
    normalizer,
    stabilizer,
    w_out,
    mlp_gain,
    w_up,
    w_down,
):
    local_heads = memory.shape[1]
    qk_width = memory.shape[2]
    model_width = mlp_gain.shape[0]
    own_rows = gather_directly(tokens, "tp", 1)
    own_f = own_rows.astype(jnp.float32)
    scaled = (own_f * norm_gain).astype(jnp.bfloat16)

    def product(weight):
        return jnp.dot(scaled, weight, preferred_element_type=jnp.float32).astype(jnp.bfloat16)

    part_query = product(w_query)
    part_key = product(w_key)
    part_value = product(w_value)
    part_gate = product(w_outgate)
    part_input = product(w_ingate)
    part_forget = product(w_forget)
    part_squares = jnp.sum(own_f * own_f, axis=1, keepdims=True)
    upper_piece = part_squares.astype(jnp.bfloat16)
    rest_one = part_squares - upper_piece.astype(jnp.float32)
    middle_piece = rest_one.astype(jnp.bfloat16)
    lower_piece = (rest_one - middle_piece.astype(jnp.float32)).astype(jnp.bfloat16)
    pieces = jnp.concatenate([upper_piece, middle_piece, lower_piece], axis=1)
    sum_query, sum_key, sum_value, sum_gate, sum_input, sum_forget, square_parts = in_one_piece(
        (part_query, part_key, part_value, part_gate, part_input, part_forget, pieces), "kv", 0, 1
    )
    squares = jnp.sum(square_parts, axis=1)
    seq_rows = sum_query.shape[0]
    rscale = lax.rsqrt(squares / model_width + EPSILON)[:, None]
    queries = (sum_query * rscale).reshape(seq_rows, local_heads, qk_width)
    keys_in = (sum_key * rscale * qk_width ** (-0.5)).reshape(seq_rows, local_heads, qk_width)
    values_in = (sum_value * rscale).reshape(seq_rows, local_heads, -1)
    out_pre = (sum_gate * rscale).reshape(seq_rows, local_heads, -1)
    head_first = lax.axis_index("tp") * local_heads
    log_in = lax.dynamic_slice_in_dim(
        sum_input * rscale, head_first, local_heads, 1
    ) + lax.dynamic_slice_in_dim(in_bias, head_first, local_heads, 0)
    forget_arg = lax.dynamic_slice_in_dim(
        sum_forget * rscale, head_first, local_heads, 1
    ) + lax.dynamic_slice_in_dim(forget_bias, head_first, local_heads, 0)
    log_forget = jax.nn.log_sigmoid(forget_arg)
    carried = log_forget + stabilizer
    stab_new = jnp.maximum(carried, log_in)
    take_new = jnp.exp(log_in - stab_new)
    keep_old = jnp.exp(carried - stab_new)
    norm_old = normalizer.reshape(seq_rows, local_heads, qk_width)
    score = jnp.sum(queries * keys_in, axis=2)
    readout = jnp.einsum("shkv,shk->shv", memory, queries, precision=lax.Precision.HIGHEST)
    numer = (take_new * score)[..., None] * values_in + keep_old[..., None] * readout
    denom = take_new * score + keep_old * jnp.sum(norm_old * queries, axis=2)
    cell = numer / jnp.maximum(jnp.abs(denom), 1.0)[..., None]
    hidden = (jax.nn.sigmoid(out_pre) * cell).reshape(seq_rows, -1).astype(jnp.bfloat16)
    memory_new = (
        keep_old[..., None, None] * memory
        + take_new[..., None, None] * keys_in[..., :, None] * values_in[..., None, :]
    )
    normalizer_new = (keep_old[..., None] * norm_old + take_new[..., None] * keys_in).reshape(
        seq_rows, -1
    )
    head_terms = jnp.dot(
        gather_directly(hidden, "kv", 0), w_out, preferred_element_type=jnp.float32
    )
    head_total = sum_at_owner(head_terms.astype(jnp.bfloat16), "tp", 1)
    middle = (tokens.astype(jnp.float32) + head_total).astype(jnp.bfloat16)
    whole_mid = gathered_by_axis(middle, ("kv", "tp"), (0, 1), 1)
    branch = sum_at_owner(channel_mix(whole_mid, mlp_gain, w_up, w_down), ("kv", "tp"), 1)
    mixed_out = (middle.astype(jnp.float32) + branch).astype(jnp.bfloat16)
    return (mixed_out, memory_new, normalizer_new, stab_new)


def solution(mesh):
    placed = (
        P(("grp", "dp"), ("kv", "tp")),
        P("kv"),
        P("kv", "tp"),
        P("kv", "tp"),
        P("kv", "tp"),
        P("kv", "tp"),
        P("kv", None),
        P("kv", None),
        P(),
        P(),
        P(("grp", "dp", "kv"), "tp", None, None),
        P(("grp", "dp", "kv"), "tp"),
        P(("grp", "dp", "kv"), "tp"),
        P("tp", "kv"),
        P(),
        P(None, ("kv", "tp")),
        P(("kv", "tp"), None),
    )
    return jax.shard_map(
        shards,
        mesh=mesh,
        in_specs=placed,
        out_specs=(
            P(("grp", "dp"), ("kv", "tp")),
            P(("grp", "dp", "kv"), "tp", None, None),
            P(("grp", "dp", "kv"), "tp"),
            P(("grp", "dp", "kv"), "tp"),
        ),
        check_vma=False,
    )
```

profile of v0, /device:TPU:65, one launch (start us, length us, event | category | flops | bytes accessed | tf_op | source)
XLA Modules:
  0.0 187.3 jit_solution(18381242777243515250)
XLA Ops:
  0.7 0.8 broadcast_in_dim.6
  1.5 44.8 %all_to_all.25 = bf16[2,128,64]{1,2,0:T(8,128)(2,1)S(1)} all-to-all(bf16[2,128,64]{1,2,0:T(8,128)(2,1)S(1)} %broadcast_in_dim.6), channel_id=1, replica_groups=mesh['grp'=2,'dp'=8,'kv'=16,'tp'=2] {'tp'}, dimensions={0} | all-to-all | bytes 65536 | tf_op jit(solution)/shard_map/all_to_all | solution.py:17
  46.3 0.7 fusion.9
  47.1 0.2 fusion
  47.3 0.7 copy-done.3
  48.0 0.2 fusion.1
  48.2 0.6 copy-done.5
  48.8 0.2 fusion.4
  49.0 0.6 copy-done.6
  49.7 0.2 fusion.5
  49.9 0.5 copy-done.10
  50.3 0.1 convolution_convert_fusion.7
  50.5 0.1 copy.108
  50.6 0.6 copy-done.11
  51.2 0.1 convolution_convert_fusion.6
  51.3 0.1 copy.109
  51.5 0.1 reduce_sum.75
  51.5 0.1 copy.90
  51.6 0.2 copy.94
  51.8 0.1 copy.95
  51.9 0.1 copy.96
  52.1 0.9 concatenate.22
  53.0 4.1 %all-to-all-start.1 = ((bf16[16,8,1555]{2,1,0:T(8,128)(2,1)}), bf16[16,8,1555]{2,1,0:T(8,128)(2,1)S(1)}, u32[]{:S(2)}, u32[]{:S(2)}) async-start(bf16[16,8,1555]{2,1,0:T(8,128)(2,1)} %concatenate.22), calls=%async_computation.1 | async-start | bytes 851968 | tf_op jit(solution)/shard_map/all_to_all | solution.py:31
  57.2 0.1 dynamic_slice.13
  57.3 0.1 copy.97
  57.4 0.1 reshape.156
  57.5 19.5 %all-to-all-done.1 = bf16[16,8,1555]{2,1,0:T(8,128)(2,1)S(1)} async-done(((bf16[16,8,1555]{2,1,0:T(8,128)(2,1)}), bf16[16,8,1555]{2,1,0:T(8,128)(2,1)S(1)}, u32[]{:S(2)}, u32[]{:S(2)}) %all-to-all-start.1) | async-done | bytes 398112 | tf_op jit(solution)/shard_map/all_to_all | solution.py:31
  77.0 0.2 slice_reduce_fusion
  77.2 0.1 slice_multiply_fusion.5
  77.3 0.1 subtract_exponential_fusion
  77.4 0.1 subtract_exponential_fusion.1
  77.5 0.1 mul.203
  77.6 0.1 mul.211
  77.7 0.1 mul.209
  77.8 0.7 multiply_add_fusion.1
  78.5 0.1 reshape.153
  78.6 0.1 reshape.167
  78.7 0.1 copy.99
  78.7 0.1 reshape.154
  78.8 0.1 multiply_reduce_fusion.2
  78.9 0.1 copy.100
  79.0 0.1 copy.98
  79.1 1.0 fusion.30
  80.1 0.1 fusion.22
  80.2 23.1 %all_to_all.26 = bf16[16,8,512]{2,1,0:T(8,128)(2,1)S(1)} all-to-all(bf16[16,8,512]{2,1,0:T(8,128)(2,1)S(1)} %broadcast_in_dim.7), channel_id=1, replica_groups=mesh['grp'=2,'dp'=8,'kv'=16,'tp'=2] {'kv'}, dimensions={0} | all-to-all | bytes 262144 | tf_op jit(solution)/shard_map/all_to_all | solution.py:17
  103.3 0.2 convolution_convert_fusion.5
  103.5 6.9 %all_to_all.27 = bf16[2,128,64]{1,2,0:T(8,128)(2,1)S(1)} all-to-all(bf16[2,128,64]{1,2,0:T(8,128)(2,1)S(1)} %bitcast.91), channel_id=1, replica_groups=mesh['grp'=2,'dp'=8,'kv'=16,'tp'=2] {'tp'}, dimensions={0} | all-to-all | bytes 65536 | tf_op jit(solution)/shard_map/all_to_all | solution.py:31
  110.4 0.7 copy-done.7
  111.1 23.2 %all-gather = bf16[2048,64]{0,1:T(8,128)(2,1)S(1)} all-gather(bf16[128,64]{0,1:T(8,128)(2,1)S(1)} %add_convert_fusion.1), channel_id=2, replica_groups=mesh['grp'=2,'dp'=8,'kv'=16,'tp'=2] {'kv'}, dimensions={0}, use_global_device_ids=true | all-gather | bytes 278528 | tf_op jit(solution)/shard_map/all_gather | solution.py:47
  134.3 8.9 %all_gather.7 = bf16[32,128,64]{1,0,2:T(8,128)(2,1)S(1)} all-gather(bf16[16,128,64]{1,0,2:T(8,128)(2,1)S(1)} %bitcast.87), channel_id=1, replica_groups=mesh['grp'=2,'dp'=8,'kv'=16,'tp'=2] {'tp'}, dimensions={0}, use_global_device_ids=true | all-gather | bytes 786432 | tf_op jit(solution)/shard_map/all_gather | solution.py:47
  143.2 0.1 convert_element_type.217
  143.3 0.2 copy.101
  143.5 0.6 copy.102
  144.2 0.3 multiply_reduce_fusion
  144.5 0.4 copy-done.9
  144.8 0.3 fusion.7
  145.2 2.0 %convolution_convert_fusion = bf16[128,2048]{1,0:T(8,128)(2,1)S(1)} fusion(bf16[256,2048]{1,0:T(8,128)(2,1)S(1)} %copy-done, bf16[128,2048]{0,1:T(8,128)(2,1)S(1)} %fusion.7, bf16[2048,256]{1,0:T(8,128)(2,1)} %param.32), kind=kOutput, calls=%fused_computation | convolution fusion | flops 268795904 | bytes 3145728 | tf_op jit(solution)/shard_map/dot_general | solution.py:64
  147.2 1.0 copy.103
  148.2 5.1 %all-to-all-start.4 = ((bf16[32,128,64]{1,2,0:T(8,128)(2,1)}), bf16[32,128,64]{1,2,0:T(8,128)(2,1)S(1)}, u32[]{:S(2)}, u32[]{:S(2)}) async-start(bf16[32,128,64]{1,2,0:T(8,128)(2,1)} %bitcast.23), calls=%async_computation.4 | async-start | bytes 1048576 | tf_op jit(solution)/shard_map/all_to_all | solution.py:31
  153.3 0.7 copy.105
  154.0 1.4 multiply_add_fusion
  155.4 31.2 %all-to-all-done.4 = bf16[32,128,64]{1,2,0:T(8,128)(2,1)S(1)} async-done(((bf16[32,128,64]{1,2,0:T(8,128)(2,1)}), bf16[32,128,64]{1,2,0:T(8,128)(2,1)S(1)}, u32[]{:S(2)}, u32[]{:S(2)}) %all-to-all-start.4) | async-done | bytes 524320 | tf_op jit(solution)/shard_map/all_to_all | solution.py:31
  186.6 0.1 convert_reduce_fusion
  186.7 0.6 add_convert_fusion
  (37 shorter events, 0.5 us)
Async XLA Ops:
  0.6 144.6 %copy-start = (bf16[256,2048]{1,0:T(8,128)(2,1)S(1)}, bf16[256,2048]{1,0:T(8,128)(2,1)}, u32[]{:S(2)}) copy-start(bf16[256,2048]{1,0:T(8,128)(2,1)} %param.33) | copy-start | bytes 3145732
  0.6 46.4 %copy-start.2 = (bf16[128,512]{1,0:T(8,128)(2,1)S(1)}, bf16[128,512]{1,0:T(8,128)(2,1)}, u32[]{:S(2)}) copy-start(bf16[128,512]{1,0:T(8,128)(2,1)} %param.21) | copy-start | bytes 393220
  47.1 0.9 copy-start.3
  48.0 0.8 copy-start.5
  48.8 0.8 copy-start.6
  49.7 0.7 copy-start.10
  50.5 0.7 copy-start.11
  52.1 5.1 %copy-start.13 = (f32[8]{0:T(128)S(1)}, f32[8]{0:T(128)}, u32[]{:S(2)}) copy-start(f32[8]{0:T(128)} %param.25) | copy-start | bytes 100
  52.1 5.2 %copy-start.14 = (f32[8]{0:T(128)S(1)}, f32[8]{0:T(128)}, u32[]{:S(2)}) copy-start(f32[8]{0:T(128)} %param.26) | copy-start | bytes 100
  52.1 5.2 %copy-start.12 = (f32[8,4]{0,1:T(4,128)S(1)}, f32[8,4]{0,1:T(4,128)}, u32[]{:S(2)}) copy-start(f32[8,4]{0,1:T(4,128)} %param.29) | copy-start | bytes 388
  52.1 5.3 %copy-start.8 = (f32[8,256]{1,0:T(8,128)S(1)}, f32[8,256]{1,0:T(8,128)}, u32[]{:S(2)}) copy-start(f32[8,256]{1,0:T(8,128)} %param.28) | copy-start | bytes 24580
  53.0 26.1 %copy-start.1 = (f32[8,4,64,128]{3,2,1,0:T(8,128)S(1)}, f32[8,4,64,128]{3,2,1,0:T(8,128)}, u32[]{:S(2)}) copy-start(f32[8,4,64,128]{3,2,1,0:T(8,128)} %param.27) | copy-start | bytes 3145732
  53.0 23.9 %all-to-all-start.1 = ((bf16[16,8,1555]{2,1,0:T(8,128)(2,1)}), bf16[16,8,1555]{2,1,0:T(8,128)(2,1)S(1)}, u32[]{:S(2)}, u32[]{:S(2)}) async-start(bf16[16,8,1555]{2,1,0:T(8,128)(2,1)} %concatenate.22), calls=%async_computation.1 | async-start | bytes 851968 | tf_op jit(solution)/shard_map/all_to_all | solution.py:31
  80.2 23.1 %copy-start.4 = (bf16[512,128]{1,0:T(8,128)(2,1)S(1)}, bf16[512,128]{1,0:T(8,128)(2,1)}, u32[]{:S(2)}) copy-start(bf16[512,128]{1,0:T(8,128)(2,1)} %param.30) | copy-start | bytes 393220
  110.4 0.7 copy-start.7
  144.1 0.7 copy-start.9
  148.2 38.4 %all-to-all-start.4 = ((bf16[32,128,64]{1,2,0:T(8,128)(2,1)}), bf16[32,128,64]{1,2,0:T(8,128)(2,1)S(1)}, u32[]{:S(2)}, u32[]{:S(2)}) async-start(bf16[32,128,64]{1,2,0:T(8,128)(2,1)} %bitcast.23), calls=%async_computation.4 | async-start | bytes 1048576 | tf_op jit(solution)/shard_map/all_to_all | solution.py:31
where the time goes:
time: 188 us; the launch traced here: 187 us
  blocking collectives  107 us (57%)
  waiting for transfers between devices  50.7 us (27%)
  local copies, waits for them, and re-layouts  10.3 us (5%)
  starting transfers between devices  9.22 us (5%)
  other arithmetic  5.06 us (3%)
  matrix products  4.26 us (2%)
    all_to_all x2, blocking collectives, copy_for_each(): return lax.all_to_all(copies, axis, split_axis=0, concat_axis=0, tiled=True)  67.9 us
    all_to_all x2, waiting for transfers between devices, sum_at_owner(): lax.all_to_all(tiles, axis, split_axis=0, concat_axis=0, tiled=True)  50.7 us
    all_gather x2, blocking collectives, gather_in_order(): tiles = lax.all_gather(tiles, axes[k], axis=0, tiled=True)  32.1 us
    all_to_all x2, starting transfers between devices, sum_at_owner(): lax.all_to_all(tiles, axis, split_axis=0, concat_axis=0, tiled=True)  9.22 us
    all_to_all x1, blocking collectives, sum_at_owner(): lax.all_to_all(tiles, axis, split_axis=0, concat_axis=0, tiled=True)  6.85 us
    unnamed x33, local copies, waits for them, and re-layouts  4.93 us
  transfers between devices with their start and end apart: 2, of which 2 were waited for; matrix products, arithmetic and copies ran while one was open for 1% of the time, Pallas kernels for 0%

commit v1 on v0

v1 whole, which is shorter than its diff:
```python
import functools

import jax
import jax.numpy as jnp
from jax import lax
from jax.experimental import pallas as pl
from jax.experimental.pallas import tpu as pltpu
from jax.sharding import PartitionSpec as P

EPSILON = 1e-06
MESH = pl.DeviceIdType.MESH
F32 = jnp.float32
BF16 = jnp.bfloat16

TWO_LEVEL = {1: 0, 2: 0, 3: 0, 4: 0, 5: 4, 6: 4, 7: 4, 8: 4}
PROJ_TREE = TWO_LEVEL
HID_TREE = TWO_LEVEL
MID_TREE = TWO_LEVEL
DOWN_TREE = TWO_LEVEL
REACH = 4


def messages(tree, n):
    half = n // 2
    out = []
    for side, last in ((1, half), (-1, n - 1 - half)):
        for k in range(1, last + 1):
            out.append((len(out), side, k, tree[k]))
    return out


def children_of(msgs, side, k):
    return [m for m in msgs if m[1] == side and m[3] == k]


def depth_below(msgs, m):
    below = children_of(msgs, m[1], m[2])
    return 1 + max(depth_below(msgs, c) for c in below) if below else 0


def level_of(tree, k):
    return 0 if k == 0 else 1 + level_of(tree, tree[k])


def kernel(
    n,
    tok,
    ngain,
    wq,
    wk,
    wv,
    wg,
    wi,
    wf,
    ib,
    fb,
    mem,
    nrm,
    stab,
    wo,
    mgain,
    wup,
    wdn,
    out,
    mem_new,
    nrm_new,
    stab_new,
    tokb,
    ngv,
    wp,
    wib,
    wfb,
    ibb,
    fbb,
    memb,
    memo,
    nrmb,
    stabb,
    wob,
    mgb,
    wupb,
    wdnb,
    pf,
    ps,
    pr,
    sf,
    ro,
    tokrow,
    hidg,
    opown,
    opsend,
    oprecv,
    midg,
    down_own,
    ds,
    dr,
    fxs,
    fxr,
    lsem,
    xs,
    xr,
    ps_s,
    ps_r,
    hid_s,
    hid_r,
    mid_s,
    mid_r,
    dn_s,
    dn_r,
):
    me = lax.axis_index("kv")
    tp = lax.axis_index("tp")
    other = 1 - tp
    rows = tokb.shape[1]
    half_ch = tokb.shape[2]
    seqs, heads, qk, vd = memb.shape
    hw = heads * qk
    vw = heads * vd
    proj = wp.shape[1]
    width = mgb.shape[0] * mgb.shape[1]
    half_rows = rows // 2

    def at(z):
        return lax.rem(z + 2 * n, n)

    barrier = pltpu.get_barrier_semaphore()
    for step in range(1, REACH + 1):
        for side in (1, -1):
            pl.semaphore_signal(barrier, inc=1, device_id={"kv": at(me + side * step)}, device_id_type=MESH)
    pl.semaphore_signal(barrier, inc=1, device_id={"tp": other}, device_id_type=MESH)

    loads = {}

    def load(name, src, dst):
        c = pltpu.make_async_copy(src, dst, lsem.at[len(loads)])
        c.start()
        loads[name] = c

    load("tok", tok, tokb.at[tp])
    load("ngain", ngain, ngv)
    load("wq", wq, wp.at[:, 0:hw])
    load("wk", wk, wp.at[:, hw : 2 * hw])
    load("wv", wv, wp.at[:, 2 * hw : 2 * hw + vw])
    load("wg", wg, wp.at[:, 2 * hw + vw : proj])
    load("wi", wi, wib)
    load("wf", wf, wfb)
    load("ib", ib, ibb)
    load("fb", fb, fbb)
    load("stab", stab, stabb)
    load("nrm", nrm, nrmb)
    load("mem", mem, memb)
    load("wo", wo, wob)
    load("mgain", mgain, mgb)
    load("wup", wup, wupb.at[tp])
    load("wdn", wdn, wdnb.at[tp])

    pl.semaphore_wait(barrier, 2 * REACH + 1)

    def to_partner(src, dst, i):
        return pltpu.make_async_remote_copy(
            src_ref=src, dst_ref=dst, send_sem=xs.at[i], recv_sem=xr.at[i], device_id={"tp": other}, device_id_type=MESH
        )

    loads["tok"].wait()
    tok_x = to_partner(tokb.at[tp], tokb.at[tp], 0)
    tok_x.start()
    sends = [tok_x]

    for name in ("ngain", "wq", "wk", "wv", "wg", "wi", "wf"):
        loads[name].wait()

    lane128 = lax.broadcasted_iota(jnp.int32, (rows, 128), 1)

    def project(which):
        t = tokb[which].astype(F32)
        gain = jnp.where(which == 0, ngv[:, 0:half_ch], ngv[:, half_ch : 2 * half_ch])
        scaled = (t * gain).astype(BF16)
        chans = pl.ds(pl.multiple_of(which * half_ch, half_ch), half_ch)
        main = jnp.dot(scaled, wp[chans, :], preferred_element_type=F32)
        gi = jnp.dot(scaled, wib[chans, :], preferred_element_type=F32)
        gf = jnp.dot(scaled, wfb[chans, :], preferred_element_type=F32)
        sq = jnp.sum(t * t, axis=1, keepdims=True)
        zeros = jnp.zeros((rows, 128 - 2 * gi.shape[1]), F32)
        gates = jnp.concatenate([gi, gf, zeros], axis=1)
        gates = jnp.where(lane128 == 2 * gi.shape[1], sq, gates)
        return main, gates

    gate_lanes = 2 * wib.shape[1]
    main, gates = project(tp)
    pf[:, :, 0:proj] = main.reshape(n, seqs, proj)
    pf[:, :, proj:] = gates.reshape(n, seqs, 128)
    tok_x.wait_recv()
    main, gates = project(other)
    pf[:, :, 0:proj] += main.reshape(n, seqs, proj)
    pf[:, :, proj:] += gates.reshape(n, seqs, 128)

    lane8 = lax.broadcasted_iota(jnp.int32, (seqs, 128), 1)

    def pack_gates(g):
        total = g[:, gate_lanes : gate_lanes + 1] + g[:, gate_lanes + 1 : gate_lanes + 2]
        upper = total.astype(BF16).astype(F32)
        return jnp.where(lane8 == gate_lanes, upper, jnp.where(lane8 == gate_lanes + 1, total - upper, g))

    def reduce_scatter(tree, own, recv, emit, send_sem, recv_sem, send_buf):
        msgs = messages(tree, n)

        def copy_of(m):
            slot, side, k, parent = m
            return pltpu.make_async_remote_copy(
                src_ref=send_buf.at[slot],
                dst_ref=recv.at[slot],
                send_sem=send_sem.at[slot],
                recv_sem=recv_sem.at[slot],
                device_id={"kv": at(me - side * (k - parent))},
                device_id_type=MESH,
            )

        order = sorted(msgs, key=lambda m: (depth_below(msgs, m), -level_of(tree, m[2]), -m[2]))
        for m in order:
            slot, side, k, parent = m
            mine = own(at(me - side * k))
            kids = children_of(msgs, side, k)
            for c in kids:
                copy_of(c).wait_recv()
            emit(slot, mine, [c[0] for c in kids])
            c = copy_of(m)
            c.start()
            sends.append(c)
        last = [m for m in msgs if m[3] == 0]

        def finish():
            for c in last:
                copy_of(c).wait_recv()
            return [c[0] for c in last]

        return finish

    def all_gather(tree, buf, send_sem, recv_sem):
        msgs = messages(tree, n)

        def copy_of(m):
            slot, side, k, parent = m
            origin = at(me - side * parent)
            return pltpu.make_async_remote_copy(
                src_ref=buf.at[origin],
                dst_ref=buf.at[origin],
                send_sem=send_sem.at[slot],
                recv_sem=recv_sem.at[slot],
                device_id={"kv": at(me + side * (k - parent))},
                device_id_type=MESH,
            )

        def arrival(m):
            slot, side, k, parent = m
            origin = at(me - side * k)
            return pltpu.make_async_remote_copy(
                src_ref=buf.at[origin],
                dst_ref=buf.at[origin],
                send_sem=send_sem.at[slot],
                recv_sem=recv_sem.at[slot],
                device_id={"kv": at(me - side * k)},
                device_id_type=MESH,
            )

        def send(m):
            c = copy_of(m)
            c.start()
            sends.append(c)

        waited = set()
        firsts = [m for m in msgs if m[3] == 0]
        for m in sorted(firsts, key=lambda m: (-depth_below(msgs, m), -m[2])):
            send(m)

        def finish():
            todo = sorted([m for m in msgs if children_of(msgs, m[1], m[2])], key=lambda m: (level_of(tree, m[2]), m[2]))
            for m in todo:
                arrival(m).wait_recv()
                waited.add(m[0])
                for c in sorted(children_of(msgs, m[1], m[2]), key=lambda c: (-depth_below(msgs, c), -c[2])):
                    send(c)
            for m in msgs:
                if m[0] not in waited:
                    arrival(m).wait_recv()

        return finish

    def own_proj(d):
        return pf[d, :, 0:proj], pf[d, :, proj:]

    def sum_proj(mine, slots):
        a, g = mine
        for s in slots:
            a = a + pr[s, :, 0:proj].astype(F32)
            g = g + pr[s, :, proj:].astype(F32)
        return a, g

    def emit_proj(slot, mine, slots):
        a, g = sum_proj(mine, slots)
        ps[slot, :, 0:proj] = a.astype(BF16)
        ps[slot, :, proj:] = pack_gates(g).astype(BF16)

    finish = reduce_scatter(PROJ_TREE, own_proj, pr, emit_proj, ps_s, ps_r, ps)

    loads["wup"].wait()
    loads["wdn"].wait()
    up_x = to_partner(wupb.at[tp], wupb.at[tp], 1)
    up_x.start()
    dn_x = to_partner(wdnb.at[tp], wdnb.at[tp], 2)
    dn_x.start()
    sends += [up_x, dn_x]
    my_rows = pl.ds(pl.multiple_of(tp * half_rows, half_rows), half_rows)
    their_rows = pl.ds(pl.multiple_of(other * half_rows, half_rows), half_rows)
    tokrow[...] = jnp.concatenate([tokb[0, my_rows, :], tokb[1, my_rows, :]], axis=1).astype(F32)
    for name in ("ib", "fb", "stab", "nrm", "mem", "wo", "mgain"):
        loads[name].wait()

    slots = finish()
    total, gate = sum_proj(own_proj(me), slots)
    sf[:, 0:proj] = total
    squares = gate[:, gate_lanes : gate_lanes + 1] + gate[:, gate_lanes + 1 : gate_lanes + 2]
    rscale = lax.rsqrt(squares / width + EPSILON)
    q = sf[:, 0:hw] * rscale
    k = sf[:, hw : 2 * hw] * rscale * qk ** (-0.5)
    v = sf[:, 2 * hw : 2 * hw + vw] * rscale
    all_heads = wib.shape[1]

    def mine_of(x, first):
        return jnp.where(tp == 0, x[:, first : first + heads], x[:, first + heads : first + 2 * heads])

    log_in = mine_of(gate, 0) * rscale + mine_of(ibb[...], 0)
    fpre = mine_of(gate, all_heads) * rscale + mine_of(fbb[...], 0)
    log_forget = jnp.minimum(fpre, 0.0) - jnp.log(1.0 + jnp.exp(-jnp.abs(fpre)))
    carried = log_forget + stabb[...]
    snew = jnp.maximum(carried, log_in)
    take = jnp.exp(log_in - snew)
    keep = jnp.exp(carried - snew)
    stab_new[...] = snew

    hlane = lax.broadcasted_iota(jnp.int32, (seqs, hw), 1) // qk

    def spread(x):
        r = jnp.broadcast_to(x[:, 0:1], (seqs, hw))
        for h in range(1, heads):
            r = jnp.where(hlane == h, x[:, h : h + 1], r)
        return r

    def per_head(x):
        return [jnp.sum(jnp.where(hlane == h, x, 0.0), axis=1, keepdims=True) for h in range(heads)]

    tk = spread(take) * k
    nrm_new[...] = spread(keep) * nrmb[...] + tk
    scores = per_head(q * k)
    nqs = per_head(nrmb[...] * q)
    qt = q.T
    for s in range(seqs):
        for h in range(heads):
            col = qt[h * qk : (h + 1) * qk, s : s + 1]
            ro[s : s + 1, h * vd : (h + 1) * vd] = jnp.sum(memb[s, h] * col, axis=0, keepdims=True)
    hidden = []
    for h in range(heads):
        ts = take[:, h : h + 1] * scores[h]
        kp = keep[:, h : h + 1]
        numer = ts * v[:, h * vd : (h + 1) * vd] + kp * ro[:, h * vd : (h + 1) * vd]
        denom = ts + kp * nqs[h]
        cell = numer / jnp.maximum(jnp.abs(denom), 1.0)
        og = sf[:, 2 * hw + vw + h * vd : 2 * hw + vw + (h + 1) * vd] * rscale
        hidg[me, :, h * vd : (h + 1) * vd] = ((1.0 / (1.0 + jnp.exp(-og))) * cell).astype(BF16)
    finish = all_gather(HID_TREE, hidg, hid_s, hid_r)

    kt = tk.T
    for s in range(seqs):
        for h in range(heads):
            col = kt[h * qk : (h + 1) * qk, s : s + 1]
            memo[s, h] = keep[s : s + 1, h : h + 1] * memb[s, h] + col * v[s : s + 1, h * vd : (h + 1) * vd]
    mem_out = pltpu.make_async_copy(memo, mem_new, lsem.at[len(loads)])
    mem_out.start()

    finish()
    gathered = hidg[...].astype(F32).reshape(rows, vw).astype(BF16)
    opown[...] = jnp.dot(gathered, wob[...], preferred_element_type=F32)
    opsend[...] = opown[their_rows, :]
    op_x = to_partner(opsend, oprecv, 3)
    op_x.start()
    sends.append(op_x)
    op_x.wait_recv()
    middle = (tokrow[...] + opown[my_rows, :] + oprecv[...]).astype(BF16)
    midg[me] = middle
    all_gather(MID_TREE, midg, mid_s, mid_r)()

    up_x.wait_recv()
    dn_x.wait_recv()
    sq_sum = jnp.zeros((half_rows, 128), F32)
    acc = [None, None]
    for j in range(n // 2):
        pair = []
        for z in (2 * j, 2 * j + 1):
            m = midg[z].astype(F32)
            sq_sum = sq_sum + m * m
            pair.append((m * mgb[z : z + 1, :]).astype(BF16))
        x = jnp.concatenate(pair, axis=1)
        for u in range(2):
            d = jnp.dot(x, wupb[u, j * 256 : (j + 1) * 256, :], preferred_element_type=F32)
            acc[u] = d if acc[u] is None else acc[u] + d
    rmid = lax.rsqrt(jnp.sum(sq_sum, axis=1, keepdims=True) / width + EPSILON)
    sqd = [jnp.square(jnp.maximum(a * rmid, 0.0)).astype(BF16) for a in acc]

    def own_down(d):
        cols = pl.ds(pl.multiple_of(d * 128, 128), 128)
        return jnp.dot(sqd[0], wdnb[0, :, cols], preferred_element_type=F32) + jnp.dot(
            sqd[1], wdnb[1, :, cols], preferred_element_type=F32
        )

    def sum_down(a, slots):
        for s in slots:
            a = a + dr[s].astype(F32)
        return a

    def emit_down(slot, mine, slots):
        ds[slot] = sum_down(mine, slots).astype(BF16)

    finish = reduce_scatter(DOWN_TREE, own_down, dr, emit_down, dn_s, dn_r, ds)
    mine = own_down(me) + midg[me].astype(F32)
    mixed = sum_down(mine, finish()).astype(F32)
    left, right = mixed[:, 0:half_ch], mixed[:, half_ch : 2 * half_ch]
    fxs[...] = jnp.where(tp == 0, right, left).astype(BF16)
    fin_x = to_partner(fxs, fxr, 4)
    fin_x.start()
    sends.append(fin_x)
    out[my_rows, :] = jnp.where(tp == 0, left, right).astype(BF16)
    fin_x.wait_recv()
    out[their_rows, :] = fxr[...]
    mem_out.wait()
    for c in sends:
        c.wait_send()


def shards(n, *args):
    (tok, ngain, wq, wk, wv, wg, wi, wf, ib, fb, mem, nrm, stab, wo, mgain, wup, wdn) = args
    rows, half_ch = tok.shape
    chans = ngain.shape[0]
    seqs, heads, qk, vd = mem.shape
    hw, vw = heads * qk, heads * vd
    proj = 2 * hw + 2 * vw
    wide = proj + 128
    width = mgain.shape[0]
    hid = wup.shape[1]
    msgs = n - 1
    any_space = pl.BlockSpec(memory_space=pl.ANY)
    vmem = pl.BlockSpec(memory_space=pltpu.VMEM)
    dma = pltpu.SemaphoreType.DMA
    out = pl.pallas_call(
        functools.partial(kernel, n),
        out_shape=(
            jax.ShapeDtypeStruct(tok.shape, BF16),
            jax.ShapeDtypeStruct(mem.shape, F32),
            jax.ShapeDtypeStruct(nrm.shape, F32),
            jax.ShapeDtypeStruct(stab.shape, F32),
        ),
        in_specs=[any_space] * 17,
        out_specs=(vmem, any_space, vmem, vmem),
        scratch_shapes=[
            pltpu.VMEM((2, rows, half_ch), BF16),
            pltpu.VMEM((1, chans), F32),
            pltpu.VMEM((chans, proj), BF16),
            pltpu.VMEM(wi.shape, BF16),
            pltpu.VMEM(wf.shape, BF16),
            pltpu.VMEM((1, ib.shape[0]), F32),
            pltpu.VMEM((1, fb.shape[0]), F32),
            pltpu.VMEM(mem.shape, F32),
            pltpu.VMEM(mem.shape, F32),
            pltpu.VMEM(nrm.shape, F32),
            pltpu.VMEM(stab.shape, F32),
            pltpu.VMEM(wo.shape, BF16),
            pltpu.VMEM((width // 128, 128), F32),
            pltpu.VMEM((2, *wup.shape), BF16),
            pltpu.VMEM((2, *wdn.shape), BF16),
            pltpu.VMEM((n, seqs, wide), F32),
            pltpu.VMEM((msgs, seqs, wide), BF16),
            pltpu.VMEM((msgs, seqs, wide), BF16),
            pltpu.VMEM((seqs, proj), F32),
            pltpu.VMEM((seqs, vw), F32),
            pltpu.VMEM((rows // 2, 128), F32),
            pltpu.VMEM((n, seqs, vw), BF16),
            pltpu.VMEM((rows, 128), F32),
            pltpu.VMEM((rows // 2, 128), F32),
            pltpu.VMEM((rows // 2, 128), F32),
            pltpu.VMEM((n, rows // 2, 128), BF16),
            pltpu.VMEM((rows // 2, 128), F32),
            pltpu.VMEM((msgs, rows // 2, 128), BF16),
            pltpu.VMEM((msgs, rows // 2, 128), BF16),
            pltpu.VMEM((rows // 2, half_ch), BF16),
            pltpu.VMEM((rows // 2, half_ch), BF16),
            dma((20,)),
            dma((5,)),
            dma((5,)),
            dma((msgs,)),
            dma((msgs,)),
            dma((msgs,)),
            dma((msgs,)),
            dma((msgs,)),
            dma((msgs,)),
            dma((msgs,)),
            dma((msgs,)),
        ],
        compiler_params=pltpu.CompilerParams(collective_id=0, has_side_effects=True, vmem_limit_bytes=40 * 2**20),
        name="cell_step",
    )(
        tok,
        ngain.reshape(1, -1),
        wq,
        wk,
        wv,
        wg,
        wi,
        wf,
        ib.reshape(1, -1),
        fb.reshape(1, -1),
        mem,
        nrm,
        stab,
        wo,
        mgain.reshape(-1, 128),
        wup,
        wdn,
    )
    return tuple(out)


def solution(mesh):
    placed = (
        P(("grp", "dp"), ("kv", "tp")),
        P("kv"),
        P("kv", "tp"),
        P("kv", "tp"),
        P("kv", "tp"),
        P("kv", "tp"),
        P("kv", None),
        P("kv", None),
        P(),
        P(),
        P(("grp", "dp", "kv"), "tp", None, None),
        P(("grp", "dp", "kv"), "tp"),
        P(("grp", "dp", "kv"), "tp"),
        P("tp", "kv"),
        P(),
        P(None, ("kv", "tp")),
        P(("kv", "tp"), None),
    )
    return jax.shard_map(
        functools.partial(shards, mesh.shape["kv"]),
        mesh=mesh,
        in_specs=placed,
        out_specs=(
            P(("grp", "dp"), ("kv", "tp")),
            P(("grp", "dp", "kv"), "tp", None, None),
            P(("grp", "dp", "kv"), "tp"),
            P(("grp", "dp", "kv"), "tp"),
        ),
        check_vma=False,
    )
```

time: 188 us -> 113 us (0.60)
  blocking collectives: 107 us -> 0 us
  Pallas kernels: 0 us -> 97.4 us
  waiting for transfers between devices: 50.7 us -> 0 us
  starting transfers between devices: 9.22 us -> 0 us
  other arithmetic: 5.06 us -> 0 us
  local copies, waits for them, and re-layouts: 10.3 us -> 14.7 us
  matrix products: 4.26 us -> 0 us
    pallas_call x0 -> x1, Pallas kernels: none -> 97.4 us  [shards(): pl.pallas_call(functools.partial(kernel, n), out_shape=(jax.ShapeDtypeStr...]
    all_to_all x3 -> x0, blocking collectives: 74.8 us -> none  [the longest x2 67.9 us: copy_for_each(): return lax.all_to_all(copies, axis, split_axis=0, concat_axis=0, tiled=True)]
    all_to_all x2 -> x0, waiting for transfers between devices: 50.7 us -> none  [sum_at_owner(): lax.all_to_all(tiles, axis, split_axis=0, concat_axis=0, tiled=True)]
    all_gather x2 -> x0, blocking collectives: 32.1 us -> none  [gather_in_order(): tiles = lax.all_gather(tiles, axes[k], axis=0, tiled=True)]
    all_to_all x2 -> x0, starting transfers between devices: 9.22 us -> none  [sum_at_owner(): lax.all_to_all(tiles, axis, split_axis=0, concat_axis=0, tiled=True)]
    unnamed x33 -> x32, local copies, waits for them, and re-layouts: 4.93 us -> 13.4 us
    dot_general x9 -> x0, matrix products: 4.26 us -> none  [the longest x1 2.02 us: channel_mix(): jnp.dot(squared, w_down, preferred_element_type=jnp.float32)]
    convert_element_type x6 -> x0, local copies, waits for them, and re-layouts: 2.22 us -> none  [the longest x1 0.99 us: channel_mix(): jnp.dot(squared, w_down, preferred_element_type=jnp.float32)]
  transfers between devices with their start and end apart: 2 -> 0, of which waited for: 2 -> 0; matrix products, arithmetic and copies ran while one was open for 1% -> 0% of each run, Pallas kernels for 0% -> 0%
where the time goes in v1:
time: 113 us
  Pallas kernels  97.4 us (86%)
  local copies, waits for them, and re-layouts  14.7 us (13%)
    pallas_call x1, Pallas kernels, shards(): pl.pallas_call(functools.partial(kernel, n), out_shape=(jax.ShapeDtypeStr...  97.4 us
    unnamed x32, local copies, waits for them, and re-layouts  13.4 us

profile of v1, /device:TPU:65, one launch (start us, length us, event | category | flops | bytes accessed | tf_op | source)
XLA Modules:
  0.0 112.9 jit_solution(15175214320402052453)
XLA Ops:
  0.6 0.0 copy-start.3
  0.6 0.8 copy.24.stab
  1.4 0.8 copy.21.tok
  2.3 0.8 copy.22.wi
  3.1 0.0 copy-start.10
  3.1 0.0 copy-start.11
  3.1 0.0 copy-start.12
  3.1 0.8 copy.23.wf
  3.9 0.0 copy-done.3
  3.9 0.0 copy-done.10
  3.9 0.0 copy-done.11
  3.9 0.0 copy-done.12
  3.9 0.0 copy-start
  4.0 1.2 %copy-done = f32[8,4,64,128]{3,2,1,0:T(8,128)S(1)} copy-done((f32[8,4,64,128]{3,2,1,0:T(8,128)S(1)}, f32[8,4,64,128]{3,2,1,0:T(8,128)}, u32[]{:S(2)}) %copy-start) | copy-done | bytes 1048600
  5.2 0.0 copy-start.1
  5.2 1.2 %copy-done.1 = bf16[2048,256]{1,0:T(8,128)(2,1)S(1)} copy-done((bf16[2048,256]{1,0:T(8,128)(2,1)S(1)}, bf16[2048,256]{1,0:T(8,128)(2,1)}, u32[]{:S(2)}) %copy-start.1) | copy-done | bytes 1048600
  6.4 0.0 copy-start.2
  6.4 1.2 %copy-done.2 = bf16[256,2048]{1,0:T(8,128)(2,1)S(1)} copy-done((bf16[256,2048]{1,0:T(8,128)(2,1)S(1)}, bf16[256,2048]{1,0:T(8,128)(2,1)}, u32[]{:S(2)}) %copy-start.2) | copy-done | bytes 1048600
  7.6 0.0 copy-start.4
  7.6 0.9 copy-done.4
  8.5 0.0 copy-start.5
  8.5 0.9 copy-done.5
  9.4 0.0 copy-start.6
  9.4 0.8 copy-done.6
  10.3 0.0 copy-start.7
  10.3 0.8 copy-done.7
  11.1 0.0 copy-start.8
  11.1 0.7 copy-done.8
  11.8 0.0 copy-start.9
  11.8 0.7 copy-done.9
  12.5 97.4 %cell_step.1 = (bf16[128,64]{1,0:T(8,128)(2,1)S(1)}, f32[8,4,64,128]{3,2,1,0:T(8,128)S(1)}, f32[8,256]{1,0:T(8,128)S(1)}, f32[8,4]{1,0:T(8,128)S(1)}) custom-call(bf16[128,64]{1,0:T(8,128)(2,1)S(1)} %copy.21.tok, f32[1,128]{1,0:T(1,128)S(1)} %bitcast.5, bf16[128,256]{1,0:T(8,128)(2,1)S(1)} %copy-done.6, bf16[128,256]{1,0:T(8,128)(2,1)S(1)} %copy-done.7, ...), custom_call_target="tpu_custom_call" | custom-call | tf_op jit(solution)/shard_map/cell_step/pallas_call | solution.py:452
  109.9 0.7 copy.25
  110.6 0.7 copy.26
  111.3 1.0 copy.29
  112.3 0.6 copy.30
Async XLA Ops:
  0.6 3.3 %copy-start.3 = (bf16[128,512]{1,0:T(8,128)(2,1)S(1)}, bf16[128,512]{1,0:T(8,128)(2,1)}, u32[]{:S(2)}) copy-start(bf16[128,512]{1,0:T(8,128)(2,1)} %wv.1) | copy-start | bytes 393220
  3.1 0.9 copy-start.10
  3.1 0.9 copy-start.11
  3.1 0.9 copy-start.12
  3.9 1.2 %copy-start = (f32[8,4,64,128]{3,2,1,0:T(8,128)S(1)}, f32[8,4,64,128]{3,2,1,0:T(8,128)}, u32[]{:S(2)}) copy-start(f32[8,4,64,128]{3,2,1,0:T(8,128)} %mem.1) | copy-start | bytes 3145732
  5.2 1.2 %copy-start.1 = (bf16[2048,256]{1,0:T(8,128)(2,1)S(1)}, bf16[2048,256]{1,0:T(8,128)(2,1)}, u32[]{:S(2)}) copy-start(bf16[2048,256]{1,0:T(8,128)(2,1)} %wup.1) | copy-start | bytes 3145732
  6.4 1.2 %copy-start.2 = (bf16[256,2048]{1,0:T(8,128)(2,1)S(1)}, bf16[256,2048]{1,0:T(8,128)(2,1)}, u32[]{:S(2)}) copy-start(bf16[256,2048]{1,0:T(8,128)(2,1)} %wdn.1) | copy-start | bytes 3145732
  7.6 0.9 copy-start.4
  8.5 0.9 copy-start.5
  9.4 0.8 copy-start.6
  10.3 0.8 copy-start.7
  11.1 0.7 copy-start.8
  11.8 0.7 copy-start.9

commit v2 on v1

--- a/solution.py
+++ b/solution.py
@@ -69,11 +69,9 @@
     ngv,
     wp,
     wib,
-    wfb,
     ibb,
     fbb,
     memb,
-    memo,
     nrmb,
     stabb,
     wob,
@@ -94,6 +92,7 @@
     down_own,
     ds,
     dr,
+    mixt,
     fxs,
     fxr,
     lsem,
@@ -111,8 +110,7 @@
     me = lax.axis_index("kv")
     tp = lax.axis_index("tp")
     other = 1 - tp
-    rows = tokb.shape[1]
-    half_ch = tokb.shape[2]
+    half_ch, rows = tokb.shape[1:]
     seqs, heads, qk, vd = memb.shape
     hw = heads * qk
     vw = heads * vd
@@ -142,8 +140,8 @@
     load("wk", wk, wp.at[:, hw : 2 * hw])
     load("wv", wv, wp.at[:, 2 * hw : 2 * hw + vw])
     load("wg", wg, wp.at[:, 2 * hw + vw : proj])
-    load("wi", wi, wib)
-    load("wf", wf, wfb)
+    load("wi", wi, wib.at[0])
+    load("wf", wf, wib.at[1])
     load("ib", ib, ibb)
     load("fb", fb, fbb)
     load("stab", stab, stabb)
@@ -169,30 +167,19 @@
     for name in ("ngain", "wq", "wk", "wv", "wg", "wi", "wf"):
         loads[name].wait()
 
+    gate_lanes = 2 * wib.shape[1]
     lane128 = lax.broadcasted_iota(jnp.int32, (rows, 128), 1)
-
-    def project(which):
-        t = tokb[which].astype(F32)
-        gain = jnp.where(which == 0, ngv[:, 0:half_ch], ngv[:, half_ch : 2 * half_ch])
-        scaled = (t * gain).astype(BF16)
-        chans = pl.ds(pl.multiple_of(which * half_ch, half_ch), half_ch)
-        main = jnp.dot(scaled, wp[chans, :], preferred_element_type=F32)
-        gi = jnp.dot(scaled, wib[chans, :], preferred_element_type=F32)
-        gf = jnp.dot(scaled, wfb[chans, :], preferred_element_type=F32)
-        sq = jnp.sum(t * t, axis=1, keepdims=True)
-        zeros = jnp.zeros((rows, 128 - 2 * gi.shape[1]), F32)
-        gates = jnp.concatenate([gi, gf, zeros], axis=1)
-        gates = jnp.where(lane128 == 2 * gi.shape[1], sq, gates)
-        return main, gates
-
-    gate_lanes = 2 * wib.shape[1]
-    main, gates = project(tp)
+    gw = jnp.concatenate(
+        [wib[0].astype(F32), wib[1].astype(F32), jnp.zeros((128 - gate_lanes, 2 * half_ch), F32)], axis=0
+    ).astype(BF16)
+    tok_x.wait_recv()
+    t = jnp.concatenate([tokb[0], tokb[1]], axis=0).astype(F32).T
+    scaled = (t * ngv[...]).astype(BF16)
+    main = jnp.dot(scaled, wp[...], preferred_element_type=F32)
+    gates = lax.dot_general(scaled, gw, (((1,), (1,)), ((), ())), preferred_element_type=F32)
     pf[:, :, 0:proj] = main.reshape(n, seqs, proj)
-    pf[:, :, proj:] = gates.reshape(n, seqs, 128)
-    tok_x.wait_recv()
-    main, gates = project(other)
-    pf[:, :, 0:proj] += main.reshape(n, seqs, proj)
-    pf[:, :, proj:] += gates.reshape(n, seqs, 128)
+    pf[:, :, proj:] = jnp.where(lane128 == gate_lanes, jnp.sum(t * t, axis=1, keepdims=True), gates).reshape(n, seqs, 128)
+    tokrow[...] = t
 
     lane8 = lax.broadcasted_iota(jnp.int32, (seqs, 128), 1)
 
@@ -311,7 +298,6 @@
     sends += [up_x, dn_x]
     my_rows = pl.ds(pl.multiple_of(tp * half_rows, half_rows), half_rows)
     their_rows = pl.ds(pl.multiple_of(other * half_rows, half_rows), half_rows)
-    tokrow[...] = jnp.concatenate([tokb[0, my_rows, :], tokb[1, my_rows, :]], axis=1).astype(F32)
     for name in ("ib", "fb", "stab", "nrm", "mem", "wo", "mgain"):
         loads[name].wait()
 
@@ -331,11 +317,11 @@
     log_in = mine_of(gate, 0) * rscale + mine_of(ibb[...], 0)
     fpre = mine_of(gate, all_heads) * rscale + mine_of(fbb[...], 0)
     log_forget = jnp.minimum(fpre, 0.0) - jnp.log(1.0 + jnp.exp(-jnp.abs(fpre)))
-    carried = log_forget + stabb[...]
+    carried = log_forget + stabb[...].T
     snew = jnp.maximum(carried, log_in)
     take = jnp.exp(log_in - snew)
     keep = jnp.exp(carried - snew)
-    stab_new[...] = snew
+    stab_new[...] = snew.T
 
     hlane = lax.broadcasted_iota(jnp.int32, (seqs, hw), 1) // qk
 
@@ -372,9 +358,7 @@
     for s in range(seqs):
         for h in range(heads):
             col = kt[h * qk : (h + 1) * qk, s : s + 1]
-            memo[s, h] = keep[s : s + 1, h : h + 1] * memb[s, h] + col * v[s : s + 1, h * vd : (h + 1) * vd]
-    mem_out = pltpu.make_async_copy(memo, mem_new, lsem.at[len(loads)])
-    mem_out.start()
+            mem_new[s, h] = keep[s : s + 1, h : h + 1] * memb[s, h] + col * v[s : s + 1, h * vd : (h + 1) * vd]
 
     finish()
     gathered = hidg[...].astype(F32).reshape(rows, vw).astype(BF16)
@@ -384,7 +368,7 @@
     op_x.start()
     sends.append(op_x)
     op_x.wait_recv()
-    middle = (tokrow[...] + opown[my_rows, :] + oprecv[...]).astype(BF16)
+    middle = (tokrow[my_rows, :] + opown[my_rows, :] + oprecv[...]).astype(BF16)
     midg[me] = middle
     all_gather(MID_TREE, midg, mid_s, mid_r)()
 
@@ -422,17 +406,29 @@
     finish = reduce_scatter(DOWN_TREE, own_down, dr, emit_down, dn_s, dn_r, ds)
     mine = own_down(me) + midg[me].astype(F32)
     mixed = sum_down(mine, finish()).astype(F32)
-    left, right = mixed[:, 0:half_ch], mixed[:, half_ch : 2 * half_ch]
-    fxs[...] = jnp.where(tp == 0, right, left).astype(BF16)
+    mixt[...] = mixed.T
+    mine = pl.ds(pl.multiple_of(tp * half_ch, half_ch), half_ch)
+    theirs = pl.ds(pl.multiple_of(other * half_ch, half_ch), half_ch)
+    fxs[...] = mixt[theirs, :].astype(BF16)
     fin_x = to_partner(fxs, fxr, 4)
     fin_x.start()
     sends.append(fin_x)
-    out[my_rows, :] = jnp.where(tp == 0, left, right).astype(BF16)
+    kept = mixt[mine, :]
     fin_x.wait_recv()
-    out[their_rows, :] = fxr[...]
-    mem_out.wait()
+    got = fxr[...].astype(F32)
+    out[...] = jnp.where(tp == 0, jnp.concatenate([kept, got], axis=1), jnp.concatenate([got, kept], axis=1)).astype(BF16)
     for c in sends:
         c.wait_send()
+
+
+def hand_over(*refs):
+    count = (len(refs) - 1) // 2
+    sems = refs[-1]
+    copies = [pltpu.make_async_copy(refs[i], refs[count + i], sems.at[i]) for i in range(count)]
+    for c in copies:
+        c.start()
+    for c in copies:
+        c.wait()
 
 
 def shards(n, *args):
@@ -452,25 +448,23 @@
     out = pl.pallas_call(
         functools.partial(kernel, n),
         out_shape=(
-            jax.ShapeDtypeStruct(tok.shape, BF16),
-            jax.ShapeDtypeStruct(mem.shape, F32),
-            jax.ShapeDtypeStruct(nrm.shape, F32),
-            jax.ShapeDtypeStruct(stab.shape, F32),
+            pltpu.VMEM((half_ch, rows), BF16),
+            pltpu.VMEM(mem.shape, F32),
+            pltpu.VMEM(nrm.shape, F32),
+            pltpu.VMEM((heads, seqs), F32),
         ),
         in_specs=[any_space] * 17,
-        out_specs=(vmem, any_space, vmem, vmem),
+        out_specs=(vmem,) * 4,
         scratch_shapes=[
-            pltpu.VMEM((2, rows, half_ch), BF16),
+            pltpu.VMEM((2, half_ch, rows), BF16),
             pltpu.VMEM((1, chans), F32),
             pltpu.VMEM((chans, proj), BF16),
-            pltpu.VMEM(wi.shape, BF16),
-            pltpu.VMEM(wf.shape, BF16),
+            pltpu.VMEM((2, wi.shape[1], chans), BF16),
             pltpu.VMEM((1, ib.shape[0]), F32),
             pltpu.VMEM((1, fb.shape[0]), F32),
             pltpu.VMEM(mem.shape, F32),
-            pltpu.VMEM(mem.shape, F32),
             pltpu.VMEM(nrm.shape, F32),
-            pltpu.VMEM(stab.shape, F32),
+            pltpu.VMEM((heads, seqs), F32),
             pltpu.VMEM(wo.shape, BF16),
             pltpu.VMEM((width // 128, 128), F32),
             pltpu.VMEM((2, *wup.shape), BF16),
@@ -480,7 +474,7 @@
             pltpu.VMEM((msgs, seqs, wide), BF16),
             pltpu.VMEM((seqs, proj), F32),
             pltpu.VMEM((seqs, vw), F32),
-            pltpu.VMEM((rows // 2, 128), F32),
+            pltpu.VMEM((rows, 128), F32),
             pltpu.VMEM((n, seqs, vw), BF16),
             pltpu.VMEM((rows, 128), F32),
             pltpu.VMEM((rows // 2, 128), F32),
@@ -489,8 +483,9 @@
             pltpu.VMEM((rows // 2, 128), F32),
             pltpu.VMEM((msgs, rows // 2, 128), BF16),
             pltpu.VMEM((msgs, rows // 2, 128), BF16),
-            pltpu.VMEM((rows // 2, half_ch), BF16),
-            pltpu.VMEM((rows // 2, half_ch), BF16),
+            pltpu.VMEM((2 * half_ch, rows // 2), F32),
+            pltpu.VMEM((half_ch, rows // 2), BF16),
+            pltpu.VMEM((half_ch, rows // 2), BF16),
             dma((20,)),
             dma((5,)),
             dma((5,)),
@@ -505,26 +500,34 @@
         ],
         compiler_params=pltpu.CompilerParams(collective_id=0, has_side_effects=True, vmem_limit_bytes=40 * 2**20),
         name="cell_step",
-    )(
-        tok,
+    )(*[pltpu.with_memory_space_constraint(x, pltpu.HBM) for x in (
+        tok.T,
         ngain.reshape(1, -1),
         wq,
         wk,
         wv,
         wg,
-        wi,
-        wf,
+        wi.T,
+        wf.T,
         ib.reshape(1, -1),
         fb.reshape(1, -1),
         mem,
         nrm,
-        stab,
+        stab.T,
         wo,
         mgain.reshape(-1, 128),
         wup,
         wdn,
-    )
-    return tuple(out)
+    )])
+    out = pl.pallas_call(
+        hand_over,
+        out_shape=tuple(jax.ShapeDtypeStruct(o.shape, o.dtype) for o in out),
+        in_specs=[vmem] * 4,
+        out_specs=(any_space,) * 4,
+        scratch_shapes=[dma((4,))],
+        name="hand_over",
+    )(*[pltpu.with_memory_space_constraint(o, pltpu.VMEM) for o in out])
+    return out[0].T, out[1], out[2], out[3].T
 
 
 def solution(mesh):

time: 113 us -> 99.5 us (0.88)
  local copies, waits for them, and re-layouts: 14.7 us -> 0 us
  Pallas kernels: 97.4 us -> 98.7 us
    unnamed x32 -> x0, local copies, waits for them, and re-layouts: 13.4 us -> none
    pallas_call x2 -> x0, local copies, waits for them, and re-layouts: 1.35 us -> none  [shards(): pl.pallas_call(functools.partial(kernel, n), out_shape=(jax.ShapeDtypeStr...]
    pallas_call x1 -> x2, Pallas kernels: 97.4 us -> 98.7 us  [the longest x1 97.7 us: shards(): pl.pallas_call(functools.partial(kernel, n), out_shape=(pltpu.VMEM((half_...]
where the time goes in v2:
time: 99.5 us; the launch traced here: 99.3 us
  Pallas kernels  98.7 us (99%)
    pallas_call x1, Pallas kernels, shards(): pl.pallas_call(functools.partial(kernel, n), out_shape=(pltpu.VMEM((half_...  97.7 us

profile of v2, /device:TPU:65, one launch (start us, length us, event | category | flops | bytes accessed | tf_op | source)
XLA Modules:
  0.0 99.3 jit_solution(16182238792208479841)
XLA Ops:
  0.6 97.7 %cell_step.1 = (bf16[64,128]{1,0:T(8,128)(2,1)S(1)}, f32[8,4,64,128]{3,2,1,0:T(8,128)S(1)}, f32[8,256]{1,0:T(8,128)S(1)}, f32[4,8]{1,0:T(4,128)S(1)}) custom-call(bf16[64,128]{1,0:T(8,128)(2,1)} %bitcast.10, f32[1,128]{1,0:T(1,128)} %bitcast.15, bf16[128,256]{1,0:T(8,128)(2,1)} %wq.1, bf16[128,256]{1,0:T(8,128)(2,1)} %wk.1, bf16[128,512]{1,0:T(8,128)(2,1)} %wv.1, ...), custom_call_target="tpu_custom_call" | custom-call | tf_op jit(solution)/shard_map/cell_step/pallas_call | solution.py:448
  98.3 1.0 %hand_over.1 = (bf16[64,128]{1,0:T(8,128)(2,1)}, f32[8,4,64,128]{3,2,1,0:T(8,128)}, f32[8,256]{1,0:T(8,128)}, f32[4,8]{1,0:T(4,128)}) custom-call(bf16[64,128]{1,0:T(8,128)(2,1)S(1)} %get-tuple-element.12.refs_0_, f32[8,4,64,128]{3,2,1,0:T(8,128)S(1)} %get-tuple-element.13.refs_1_, f32[8,256]{1,0:T(8,128)S(1)} %get-tuple-element.14.refs_2_, ...), custom_call_target="tpu_custom_call" | custom-call | tf_op jit(solution)/shard_map/hand_over/pallas_call | solution.py:522

commit v3 on v2

--- a/solution.py
+++ b/solution.py
@@ -17,7 +17,6 @@
 HID_TREE = TWO_LEVEL
 MID_TREE = TWO_LEVEL
 DOWN_TREE = TWO_LEVEL
-REACH = 4
 
 
 def messages(tree, n):
@@ -89,10 +88,10 @@
     opsend,
     oprecv,
     midg,
-    down_own,
     ds,
     dr,
-    mixt,
+    fs,
+    fr,
     fxs,
     fxr,
     lsem,
@@ -106,6 +105,9 @@
     mid_r,
     dn_s,
     dn_r,
+    fs_s,
+    fr_r,
+    near,
 ):
     me = lax.axis_index("kv")
     tp = lax.axis_index("tp")
@@ -122,10 +124,16 @@
         return lax.rem(z + 2 * n, n)
 
     barrier = pltpu.get_barrier_semaphore()
-    for step in range(1, REACH + 1):
+    for side in (1, -1):
+        pl.semaphore_signal(barrier, inc=1, device_id={"kv": at(me + side)}, device_id_type=MESH)
+    pl.semaphore_signal(barrier, inc=1, device_id={"tp": other}, device_id_type=MESH)
+
+    def tell(i, step):
         for side in (1, -1):
-            pl.semaphore_signal(barrier, inc=1, device_id={"kv": at(me + side * step)}, device_id_type=MESH)
-    pl.semaphore_signal(barrier, inc=1, device_id={"tp": other}, device_id_type=MESH)
+            pl.semaphore_signal(near.at[i], inc=1, device_id={"kv": at(me + side * step)}, device_id_type=MESH)
+
+    def hear(i):
+        pl.semaphore_wait(near.at[i], 2)
 
     loads = {}
 
@@ -152,7 +160,8 @@
     load("wup", wup, wupb.at[tp])
     load("wdn", wdn, wdnb.at[tp])
 
-    pl.semaphore_wait(barrier, 2 * REACH + 1)
+    pl.semaphore_wait(barrier, 3)
+    tell(0, 1)
 
     def to_partner(src, dst, i):
         return pltpu.make_async_remote_copy(
@@ -172,6 +181,8 @@
     gw = jnp.concatenate(
         [wib[0].astype(F32), wib[1].astype(F32), jnp.zeros((128 - gate_lanes, 2 * half_ch), F32)], axis=0
     ).astype(BF16)
+    hear(0)
+    tell(1, 2)
     tok_x.wait_recv()
     t = jnp.concatenate([tokb[0], tokb[1]], axis=0).astype(F32).T
     scaled = (t * ngv[...]).astype(BF16)
@@ -188,39 +199,29 @@
         upper = total.astype(BF16).astype(F32)
         return jnp.where(lane8 == gate_lanes, upper, jnp.where(lane8 == gate_lanes + 1, total - upper, g))
 
-    def reduce_scatter(tree, own, recv, emit, send_sem, recv_sem, send_buf):
+    def reduce_scatter(tree, own, emit, copies_of):
         msgs = messages(tree, n)
-
-        def copy_of(m):
-            slot, side, k, parent = m
-            return pltpu.make_async_remote_copy(
-                src_ref=send_buf.at[slot],
-                dst_ref=recv.at[slot],
-                send_sem=send_sem.at[slot],
-                recv_sem=recv_sem.at[slot],
-                device_id={"kv": at(me - side * (k - parent))},
-                device_id_type=MESH,
-            )
-
         order = sorted(msgs, key=lambda m: (depth_below(msgs, m), -level_of(tree, m[2]), -m[2]))
         for m in order:
             slot, side, k, parent = m
             mine = own(at(me - side * k))
             kids = children_of(msgs, side, k)
             for c in kids:
-                copy_of(c).wait_recv()
-            emit(slot, mine, [c[0] for c in kids])
-            c = copy_of(m)
-            c.start()
-            sends.append(c)
-        last = [m for m in msgs if m[3] == 0]
-
-        def finish():
-            for c in last:
-                copy_of(c).wait_recv()
-            return [c[0] for c in last]
-
-        return finish
+                copies_of(c)[0].wait_recv()
+            emit(m, mine, [c[0] for c in kids])
+            for c in copies_of(m):
+                c.start()
+                sends.append(c)
+        return [m for m in msgs if m[3] == 0]
+
+    def along(m, src, dst, send_sem, recv_sem, core=None):
+        slot, side, k, parent = m
+        where = {"kv": at(me - side * (k - parent))}
+        if core is not None:
+            where["tp"] = core
+        return pltpu.make_async_remote_copy(
+            src_ref=src, dst_ref=dst, send_sem=send_sem, recv_sem=recv_sem, device_id=where, device_id_type=MESH
+        )
 
     def all_gather(tree, buf, send_sem, recv_sem):
         msgs = messages(tree, n)
@@ -272,6 +273,8 @@
 
         return finish
 
+    hear(1)
+
     def own_proj(d):
         return pf[d, :, 0:proj], pf[d, :, proj:]
 
@@ -282,12 +285,17 @@
             g = g + pr[s, :, proj:].astype(F32)
         return a, g
 
-    def emit_proj(slot, mine, slots):
+    def emit_proj(m, mine, slots):
+        slot = m[0]
         a, g = sum_proj(mine, slots)
         ps[slot, :, 0:proj] = a.astype(BF16)
         ps[slot, :, proj:] = pack_gates(g).astype(BF16)
 
-    finish = reduce_scatter(PROJ_TREE, own_proj, pr, emit_proj, ps_s, ps_r, ps)
+    def proj_copies(m):
+        i = m[0]
+        return [along(m, ps.at[i], pr.at[i], ps_s.at[i], ps_r.at[i])]
+
+    last = reduce_scatter(PROJ_TREE, own_proj, emit_proj, proj_copies)
 
     loads["wup"].wait()
     loads["wdn"].wait()
@@ -301,7 +309,9 @@
     for name in ("ib", "fb", "stab", "nrm", "mem", "wo", "mgain"):
         loads[name].wait()
 
-    slots = finish()
+    for m in last:
+        proj_copies(m)[0].wait_recv()
+    slots = [m[0] for m in last]
     total, gate = sum_proj(own_proj(me), slots)
     sf[:, 0:proj] = total
     squares = gate[:, gate_lanes : gate_lanes + 1] + gate[:, gate_lanes + 1 : gate_lanes + 2]
@@ -400,23 +410,48 @@
             a = a + dr[s].astype(F32)
         return a
 
-    def emit_down(slot, mine, slots):
-        ds[slot] = sum_down(mine, slots).astype(BF16)
-
-    finish = reduce_scatter(DOWN_TREE, own_down, dr, emit_down, dn_s, dn_r, ds)
-    mine = own_down(me) + midg[me].astype(F32)
-    mixed = sum_down(mine, finish()).astype(F32)
-    mixt[...] = mixed.T
-    mine = pl.ds(pl.multiple_of(tp * half_ch, half_ch), half_ch)
-    theirs = pl.ds(pl.multiple_of(other * half_ch, half_ch), half_ch)
-    fxs[...] = mixt[theirs, :].astype(BF16)
+    def halves(a):
+        return [
+            jnp.concatenate([a[0:quarter, h : h + half_ch], a[quarter : 2 * quarter, h : h + half_ch]], axis=1)
+            for h in (0, half_ch)
+        ]
+
+    quarter = half_rows // 2
+    msgs_n = n - 1
+
+    def emit_down(m, mine, slots):
+        a = sum_down(mine, slots)
+        if m[3] == 0:
+            fs[m[0], 0], fs[m[0], 1] = [x.astype(BF16) for x in halves(a)]
+        else:
+            ds[m[0]] = a.astype(BF16)
+
+    def down_copies(m):
+        i = m[0]
+        if m[3] == 0:
+            return [
+                along(m, fs.at[i, c], fr.at[tp, i], fs_s.at[2 * i + c], fr_r.at[tp * msgs_n + i], c) for c in range(2)
+            ]
+        return [along(m, ds.at[i], dr.at[i], dn_s.at[i], dn_r.at[i])]
+
+    last = reduce_scatter(DOWN_TREE, own_down, emit_down, down_copies)
+    left, right = halves(own_down(me) + midg[me].astype(F32))
+    fxs[...] = jnp.where(tp == 0, right, left)
     fin_x = to_partner(fxs, fxr, 4)
     fin_x.start()
     sends.append(fin_x)
-    kept = mixt[mine, :]
     fin_x.wait_recv()
-    got = fxr[...].astype(F32)
-    out[...] = jnp.where(tp == 0, jnp.concatenate([kept, got], axis=1), jnp.concatenate([got, kept], axis=1)).astype(BF16)
+    sums = [jnp.where(tp == 0, left, right), fxr[...]]
+    sums = [jnp.where(tp == 0, sums[0], sums[1]), jnp.where(tp == 0, sums[1], sums[0])]
+    for m in last:
+        for r in range(2):
+            i = m[0]
+            along(m, fs.at[i, r], fr.at[r, i], fs_s.at[2 * i + r], fr_r.at[r * msgs_n + i], r).wait_recv()
+            sums[r] = sums[r] + fr[r, i].astype(F32)
+    flat = jnp.concatenate(sums, axis=0).T
+    out[...] = jnp.concatenate(
+        [flat[h : h + half_ch, r : r + quarter] for r in (0, quarter) for h in (0, half_ch)], axis=1
+    ).astype(BF16)
     for c in sends:
         c.wait_send()
 
@@ -480,12 +515,12 @@
             pltpu.VMEM((rows // 2, 128), F32),
             pltpu.VMEM((rows // 2, 128), F32),
             pltpu.VMEM((n, rows // 2, 128), BF16),
-            pltpu.VMEM((rows // 2, 128), F32),
             pltpu.VMEM((msgs, rows // 2, 128), BF16),
             pltpu.VMEM((msgs, rows // 2, 128), BF16),
-            pltpu.VMEM((2 * half_ch, rows // 2), F32),
-            pltpu.VMEM((half_ch, rows // 2), BF16),
-            pltpu.VMEM((half_ch, rows // 2), BF16),
+            pltpu.VMEM((msgs, 2, rows // 4, 128), BF16),
+            pltpu.VMEM((2, msgs, rows // 4, 128), BF16),
+            pltpu.VMEM((rows // 4, 128), F32),
+            pltpu.VMEM((rows // 4, 128), F32),
             dma((20,)),
             dma((5,)),
             dma((5,)),
@@ -497,6 +532,9 @@
             dma((msgs,)),
             dma((msgs,)),
             dma((msgs,)),
+            dma((2 * msgs,)),
+            dma((2 * msgs,)),
+            pltpu.SemaphoreType.REGULAR((2,)),
         ],
         compiler_params=pltpu.CompilerParams(collective_id=0, has_side_effects=True, vmem_limit_bytes=40 * 2**20),
         name="cell_step",

time: 99.5 us -> 98.7 us (level)
  Pallas kernels: 98.7 us -> 97 us
    pallas_call x1, Pallas kernels: 97.7 us -> 96 us  [shards(): pl.pallas_call(functools.partial(kernel, n), out_shape=(pltpu.VMEM((half_...]
where the time goes in v3:
time: 98.7 us; the launch traced here: 97.7 us
  Pallas kernels  97 us (98%)
    pallas_call x1, Pallas kernels, shards(): pl.pallas_call(functools.partial(kernel, n), out_shape=(pltpu.VMEM((half_...  96 us

profile of v3, /device:TPU:65, one launch (start us, length us, event | category | flops | bytes accessed | tf_op | source)
XLA Modules:
  0.0 97.7 jit_solution(7601773837287224461)
XLA Ops:
  0.6 96.0 %cell_step.1 = (bf16[64,128]{1,0:T(8,128)(2,1)S(1)}, f32[8,4,64,128]{3,2,1,0:T(8,128)S(1)}, f32[8,256]{1,0:T(8,128)S(1)}, f32[4,8]{1,0:T(4,128)S(1)}) custom-call(bf16[64,128]{1,0:T(8,128)(2,1)} %bitcast.10, f32[1,128]{1,0:T(1,128)} %bitcast.15, bf16[128,256]{1,0:T(8,128)(2,1)} %wq.1, bf16[128,256]{1,0:T(8,128)(2,1)} %wk.1, bf16[128,512]{1,0:T(8,128)(2,1)} %wv.1, ...), custom_call_target="tpu_custom_call" | custom-call | tf_op jit(solution)/shard_map/cell_step/pallas_call | solution.py:483
  96.7 1.0 %hand_over.1 = (bf16[64,128]{1,0:T(8,128)(2,1)}, f32[8,4,64,128]{3,2,1,0:T(8,128)}, f32[8,256]{1,0:T(8,128)}, f32[4,8]{1,0:T(4,128)}) custom-call(bf16[64,128]{1,0:T(8,128)(2,1)S(1)} %get-tuple-element.12.refs_0_, f32[8,4,64,128]{3,2,1,0:T(8,128)S(1)} %get-tuple-element.13.refs_1_, f32[8,256]{1,0:T(8,128)S(1)} %get-tuple-element.14.refs_2_, ...), custom_call_target="tpu_custom_call" | custom-call | tf_op jit(solution)/shard_map/hand_over/pallas_call | solution.py:560

commit v4 on v3

--- a/solution.py
+++ b/solution.py
@@ -14,7 +14,7 @@
 
 TWO_LEVEL = {1: 0, 2: 0, 3: 0, 4: 0, 5: 4, 6: 4, 7: 4, 8: 4}
 PROJ_TREE = TWO_LEVEL
-HID_TREE = TWO_LEVEL
+REACH = 4
 MID_TREE = TWO_LEVEL
 DOWN_TREE = TWO_LEVEL
 
@@ -43,6 +43,7 @@
 
 def kernel(
     n,
+    columns,
     tok,
     ngain,
     wq,
@@ -83,10 +84,11 @@
     sf,
     ro,
     tokrow,
+    tst,
+    tokx,
+    tfwd,
+    hid_own,
     hidg,
-    opown,
-    opsend,
-    oprecv,
     midg,
     ds,
     dr,
@@ -107,10 +109,12 @@
     dn_r,
     fs_s,
     fr_r,
-    near,
+    pre_s,
+    pre_r,
 ):
     me = lax.axis_index("kv")
     tp = lax.axis_index("tp")
+    column = lax.axis_index("dp")
     other = 1 - tp
     half_ch, rows = tokb.shape[1:]
     seqs, heads, qk, vd = memb.shape
@@ -119,21 +123,18 @@
     proj = wp.shape[1]
     width = mgb.shape[0] * mgb.shape[1]
     half_rows = rows // 2
+    wo_rows = wob.shape[1]
 
     def at(z):
         return lax.rem(z + 2 * n, n)
 
     barrier = pltpu.get_barrier_semaphore()
-    for side in (1, -1):
-        pl.semaphore_signal(barrier, inc=1, device_id={"kv": at(me + side)}, device_id_type=MESH)
+    for step in range(1, REACH + 1):
+        for side in (1, -1):
+            pl.semaphore_signal(barrier, inc=1, device_id={"kv": at(me + side * step)}, device_id_type=MESH)
     pl.semaphore_signal(barrier, inc=1, device_id={"tp": other}, device_id_type=MESH)
-
-    def tell(i, step):
-        for side in (1, -1):
-            pl.semaphore_signal(near.at[i], inc=1, device_id={"kv": at(me + side * step)}, device_id_type=MESH)
-
-    def hear(i):
-        pl.semaphore_wait(near.at[i], 2)
+    for step in range(1, columns):
+        pl.semaphore_signal(barrier, inc=1, device_id={"dp": lax.rem(column + step, columns)}, device_id_type=MESH)
 
     loads = {}
 
@@ -155,13 +156,12 @@
     load("stab", stab, stabb)
     load("nrm", nrm, nrmb)
     load("mem", mem, memb)
-    load("wo", wo, wob)
+    load("wo", wo, wob.at[tp, :, 0:128])
     load("mgain", mgain, mgb)
     load("wup", wup, wupb.at[tp])
     load("wdn", wdn, wdnb.at[tp])
 
-    pl.semaphore_wait(barrier, 3)
-    tell(0, 1)
+    pl.semaphore_wait(barrier, 2 * REACH + columns)
 
     def to_partner(src, dst, i):
         return pltpu.make_async_remote_copy(
@@ -181,8 +181,6 @@
     gw = jnp.concatenate(
         [wib[0].astype(F32), wib[1].astype(F32), jnp.zeros((128 - gate_lanes, 2 * half_ch), F32)], axis=0
     ).astype(BF16)
-    hear(0)
-    tell(1, 2)
     tok_x.wait_recv()
     t = jnp.concatenate([tokb[0], tokb[1]], axis=0).astype(F32).T
     scaled = (t * ngv[...]).astype(BF16)
@@ -190,7 +188,7 @@
     gates = lax.dot_general(scaled, gw, (((1,), (1,)), ((), ())), preferred_element_type=F32)
     pf[:, :, 0:proj] = main.reshape(n, seqs, proj)
     pf[:, :, proj:] = jnp.where(lane128 == gate_lanes, jnp.sum(t * t, axis=1, keepdims=True), gates).reshape(n, seqs, 128)
-    tokrow[...] = t
+    tokrow[...] = t.reshape(n, seqs, 2 * half_ch)
 
     lane8 = lax.broadcasted_iota(jnp.int32, (seqs, 128), 1)
 
@@ -199,13 +197,16 @@
         upper = total.astype(BF16).astype(F32)
         return jnp.where(lane8 == gate_lanes, upper, jnp.where(lane8 == gate_lanes + 1, total - upper, g))
 
-    def reduce_scatter(tree, own, emit, copies_of):
+    def reduce_scatter(tree, own, emit, copies_of, before_relays=None):
         msgs = messages(tree, n)
         order = sorted(msgs, key=lambda m: (depth_below(msgs, m), -level_of(tree, m[2]), -m[2]))
         for m in order:
             slot, side, k, parent = m
             mine = own(at(me - side * k))
             kids = children_of(msgs, side, k)
+            if kids and before_relays is not None:
+                before_relays()
+                before_relays = None
             for c in kids:
                 copies_of(c)[0].wait_recv()
             emit(m, mine, [c[0] for c in kids])
@@ -273,7 +274,67 @@
 
         return finish
 
-    hear(1)
+    stride = n // 4
+    piece = pl.ds(pl.multiple_of(column * (wo_rows // columns), wo_rows // columns), wo_rows // columns)
+    parity = lax.rem(me, 2)
+    mine_offset = jnp.where(tp == parity, 0, -1)
+
+    def lanes(slot):
+        return pl.ds(slot * 128, 128)
+
+    def hop(src, dst, i, step, side="kv"):
+        where = at(me + step) if side == "kv" else lax.rem(column + step, columns)
+        return pltpu.make_async_remote_copy(
+            src_ref=src, dst_ref=dst, send_sem=pre_s.at[i], recv_sem=pre_r.at[i], device_id={side: where}, device_id_type=MESH
+        )
+
+    def piece_hop(source, slot, i, step):
+        return hop(wob.at[tp, piece, lanes(source)], wob.at[tp, piece, lanes(slot)], i, step)
+
+    for i, step in enumerate((stride, -stride, 2 * stride)):
+        for b in range(2):
+            tst[i, b] = tokrow[at(me + step + mine_offset + 2 * b)]
+    loads["wo"].wait()
+    pre = {
+        "w_up": piece_hop(0, 3, 0, stride),
+        "w_dn": piece_hop(0, 1, 1, -stride),
+        "t_up": hop(tst.at[0], tokx.at[3], 2, stride),
+        "t_dn": hop(tst.at[1], tokx.at[1], 3, -stride),
+        "t_on": hop(tst.at[2], tfwd, 4, stride),
+        "w_fw": piece_hop(3, 2, 5, stride),
+        "t_fw": hop(tfwd, tokx.at[2], 6, stride),
+    }
+
+    def begin(c):
+        c.start()
+        sends.append(c)
+
+    for name in ("w_up", "w_dn", "t_up", "t_dn", "t_on"):
+        begin(pre[name])
+    wo_x = to_partner(wob.at[tp, :, lanes(0)], wob.at[tp, :, lanes(0)], 3)
+    begin(wo_x)
+
+    def forward_on():
+        pre["w_up"].wait_recv()
+        pre["t_on"].wait_recv()
+        begin(pre["w_fw"])
+        begin(pre["t_fw"])
+
+    def to_columns():
+        pre["w_dn"].wait_recv()
+        pre["w_fw"].wait_recv()
+        for step in range(1, columns):
+            begin(column_copy(step))
+
+    def column_copy(step):
+        part = wob.at[tp, piece, 128:512]
+        return hop(part, part, 7 + step, step, "dp")
+
+    def column_arrival(step):
+        rows_there = wo_rows // columns
+        theirs = pl.ds(pl.multiple_of(lax.rem(column - step + columns, columns) * rows_there, rows_there), rows_there)
+        part = wob.at[tp, theirs, 128:512]
+        return hop(part, part, 7 + step, step, "dp")
 
     def own_proj(d):
         return pf[d, :, 0:proj], pf[d, :, proj:]
@@ -295,7 +356,8 @@
         i = m[0]
         return [along(m, ps.at[i], pr.at[i], ps_s.at[i], ps_r.at[i])]
 
-    last = reduce_scatter(PROJ_TREE, own_proj, emit_proj, proj_copies)
+    last = reduce_scatter(PROJ_TREE, own_proj, emit_proj, proj_copies, forward_on)
+    to_columns()
 
     loads["wup"].wait()
     loads["wdn"].wait()
@@ -304,9 +366,7 @@
     dn_x = to_partner(wdnb.at[tp], wdnb.at[tp], 2)
     dn_x.start()
     sends += [up_x, dn_x]
-    my_rows = pl.ds(pl.multiple_of(tp * half_rows, half_rows), half_rows)
-    their_rows = pl.ds(pl.multiple_of(other * half_rows, half_rows), half_rows)
-    for name in ("ib", "fb", "stab", "nrm", "mem", "wo", "mgain"):
+    for name in ("ib", "fb", "stab", "nrm", "mem", "mgain"):
         loads[name].wait()
 
     for m in last:
@@ -361,8 +421,36 @@
         denom = ts + kp * nqs[h]
         cell = numer / jnp.maximum(jnp.abs(denom), 1.0)
         og = sf[:, 2 * hw + vw + h * vd : 2 * hw + vw + (h + 1) * vd] * rscale
-        hidg[me, :, h * vd : (h + 1) * vd] = ((1.0 / (1.0 + jnp.exp(-og))) * cell).astype(BF16)
-    finish = all_gather(HID_TREE, hidg, hid_s, hid_r)
+        hid_own[:, h * vd : (h + 1) * vd] = ((1.0 / (1.0 + jnp.exp(-og))) * cell).astype(BF16)
+
+    def hid_hop(i, slot, step):
+        return pltpu.make_async_remote_copy(
+            src_ref=hid_own,
+            dst_ref=hidg.at[slot, tp],
+            send_sem=hid_s.at[i],
+            recv_sem=hid_r.at[2 * slot + tp],
+            device_id={"kv": at(me + step), "tp": parity},
+            device_id_type=MESH,
+        )
+
+    for i, (slot, step) in enumerate(((1, -2), (0, 1), (1, -1))):
+        begin(hid_hop(i, slot, step))
+    own_hid = pltpu.make_async_remote_copy(
+        src_ref=hid_own,
+        dst_ref=hidg.at[0, tp],
+        send_sem=hid_s.at[3],
+        recv_sem=hid_r.at[tp],
+        device_id={"tp": other},
+        device_id_type=MESH,
+    )
+
+    @pl.when(tp != parity)
+    def _():
+        own_hid.start()
+
+    @pl.when(tp == parity)
+    def _():
+        hidg[0, tp] = hid_own[...]
 
     kt = tk.T
     for s in range(seqs):
@@ -370,32 +458,76 @@
             col = kt[h * qk : (h + 1) * qk, s : s + 1]
             mem_new[s, h] = keep[s : s + 1, h : h + 1] * memb[s, h] + col * v[s : s + 1, h * vd : (h + 1) * vd]
 
-    finish()
-    gathered = hidg[...].astype(F32).reshape(rows, vw).astype(BF16)
-    opown[...] = jnp.dot(gathered, wob[...], preferred_element_type=F32)
-    opsend[...] = opown[their_rows, :]
-    op_x = to_partner(opsend, oprecv, 3)
-    op_x.start()
-    sends.append(op_x)
-    op_x.wait_recv()
-    middle = (tokrow[my_rows, :] + opown[my_rows, :] + oprecv[...]).astype(BF16)
-    midg[me] = middle
+    for step in range(1, columns):
+        column_arrival(step).wait_recv()
+    far = wob.at[tp, :, 128:512]
+    far_x = to_partner(far, far, 4)
+    begin(far_x)
+    wo_x.wait_recv()
+    for name in ("t_up", "t_dn", "t_fw"):
+        pre[name].wait_recv()
+
+    def hid_arrival(slot, core):
+        pltpu.make_async_remote_copy(
+            src_ref=hid_own,
+            dst_ref=hidg.at[slot, core],
+            send_sem=hid_s.at[0],
+            recv_sem=hid_r.at[2 * slot + core],
+            device_id={"tp": other},
+            device_id_type=MESH,
+        ).wait_recv()
+
+    for i in range(2):
+        tokx[0, i] = tokrow[at(me + mine_offset + 2 * i)]
+    far_x.wait_recv()
+
+    @pl.when(tp != parity)
+    def _():
+        own_hid.wait_send()
+        hid_arrival(0, tp)
+
+    hid_arrival(0, other)
+    for core in range(2):
+        hid_arrival(1, core)
+    left_rows = jnp.concatenate(
+        [jnp.concatenate([hidg[i, h].astype(F32) for h in range(2)], axis=1) for i in range(2)], axis=0
+    ).astype(BF16)
+    added = jnp.dot(left_rows[:, 0:vw], wob[0], preferred_element_type=F32) + jnp.dot(
+        left_rows[:, vw : 2 * vw], wob[1], preferred_element_type=F32
+    )
+    for slot in range(4):
+        cols = lax.rem(me // 4 + slot, 4)
+        block = added[:, slot * 128 : (slot + 1) * 128].reshape(2, seqs, 128) + tokx[slot]
+        midg[me, :, :, pl.ds(pl.multiple_of(cols * 128, 128), 128)] = block.astype(BF16)
     all_gather(MID_TREE, midg, mid_s, mid_r)()
 
     up_x.wait_recv()
     dn_x.wait_recv()
-    sq_sum = jnp.zeros((half_rows, 128), F32)
+    blocks = half_rows // seqs
+
+    def place(group, m):
+        z = tp + 2 * m
+        offset = lax.rem(z - group + 1 + n, 4) - 1
+        return at(z - offset), lax.div(offset + 1, 2)
+
+    sq_sum = jnp.zeros((half_rows, 512), F32)
     acc = [None, None]
-    for j in range(n // 2):
-        pair = []
-        for z in (2 * j, 2 * j + 1):
-            m = midg[z].astype(F32)
-            sq_sum = sq_sum + m * m
-            pair.append((m * mgb[z : z + 1, :]).astype(BF16))
-        x = jnp.concatenate(pair, axis=1)
-        for u in range(2):
-            d = jnp.dot(x, wupb[u, j * 256 : (j + 1) * 256, :], preferred_element_type=F32)
-            acc[u] = d if acc[u] is None else acc[u] + d
+    for group in range(4):
+        parts = []
+        for m in range(blocks):
+            z, half = place(group, m)
+            parts.append(midg[z, half].astype(F32))
+        x = jnp.concatenate(parts, axis=0)
+        sq_sum = sq_sum + x * x
+        for j in range(0, 4, 2):
+            chans = [group + 4 * (j + i) for i in range(2)]
+            xs_in = jnp.concatenate(
+                [x[:, (j + i) * 128 : (j + i + 1) * 128] * mgb[c : c + 1, :] for i, c in enumerate(chans)], axis=1
+            ).astype(BF16)
+            for u in range(2):
+                w = jnp.concatenate([wupb[u, c * 128 : (c + 1) * 128, :] for c in chans], axis=0)
+                d = jnp.dot(xs_in, w, preferred_element_type=F32)
+                acc[u] = d if acc[u] is None else acc[u] + d
     rmid = lax.rsqrt(jnp.sum(sq_sum, axis=1, keepdims=True) / width + EPSILON)
     sqd = [jnp.square(jnp.maximum(a * rmid, 0.0)).astype(BF16) for a in acc]
 
@@ -435,9 +567,13 @@
         return [along(m, ds.at[i], dr.at[i], dn_s.at[i], dn_r.at[i])]
 
     last = reduce_scatter(DOWN_TREE, own_down, emit_down, down_copies)
-    left, right = halves(own_down(me) + midg[me].astype(F32))
+    own_mid = []
+    for m in range(blocks):
+        z, half = place(lax.rem(me, 4), m)
+        own_mid.append(midg[z, half, :, pl.ds(pl.multiple_of(me // 4 * 128, 128), 128)].astype(F32))
+    left, right = halves(own_down(me) + jnp.concatenate(own_mid, axis=0))
     fxs[...] = jnp.where(tp == 0, right, left)
-    fin_x = to_partner(fxs, fxr, 4)
+    fin_x = to_partner(fxs, fxr, 5)
     fin_x.start()
     sends.append(fin_x)
     fin_x.wait_recv()
@@ -448,10 +584,10 @@
             i = m[0]
             along(m, fs.at[i, r], fr.at[r, i], fs_s.at[2 * i + r], fr_r.at[r * msgs_n + i], r).wait_recv()
             sums[r] = sums[r] + fr[r, i].astype(F32)
-    flat = jnp.concatenate(sums, axis=0).T
-    out[...] = jnp.concatenate(
-        [flat[h : h + half_ch, r : r + quarter] for r in (0, quarter) for h in (0, half_ch)], axis=1
-    ).astype(BF16)
+    flat = jnp.concatenate(
+        [sums[r][m * seqs : (m + 1) * seqs] for m in range(blocks // 2) for r in range(2)], axis=0
+    ).T
+    out[...] = jnp.concatenate([flat[0:half_ch], flat[half_ch : 2 * half_ch]], axis=1).astype(BF16)
     for c in sends:
         c.wait_send()
 
@@ -466,7 +602,7 @@
         c.wait()
 
 
-def shards(n, *args):
+def shards(n, columns, *args):
     (tok, ngain, wq, wk, wv, wg, wi, wf, ib, fb, mem, nrm, stab, wo, mgain, wup, wdn) = args
     rows, half_ch = tok.shape
     chans = ngain.shape[0]
@@ -481,7 +617,7 @@
     vmem = pl.BlockSpec(memory_space=pltpu.VMEM)
     dma = pltpu.SemaphoreType.DMA
     out = pl.pallas_call(
-        functools.partial(kernel, n),
+        functools.partial(kernel, n, columns),
         out_shape=(
             pltpu.VMEM((half_ch, rows), BF16),
             pltpu.VMEM(mem.shape, F32),
@@ -500,7 +636,7 @@
             pltpu.VMEM(mem.shape, F32),
             pltpu.VMEM(nrm.shape, F32),
             pltpu.VMEM((heads, seqs), F32),
-            pltpu.VMEM(wo.shape, BF16),
+            pltpu.VMEM((2, wo.shape[0], 512), BF16),
             pltpu.VMEM((width // 128, 128), F32),
             pltpu.VMEM((2, *wup.shape), BF16),
             pltpu.VMEM((2, *wdn.shape), BF16),
@@ -509,12 +645,13 @@
             pltpu.VMEM((msgs, seqs, wide), BF16),
             pltpu.VMEM((seqs, proj), F32),
             pltpu.VMEM((seqs, vw), F32),
-            pltpu.VMEM((rows, 128), F32),
-            pltpu.VMEM((n, seqs, vw), BF16),
-            pltpu.VMEM((rows, 128), F32),
-            pltpu.VMEM((rows // 2, 128), F32),
-            pltpu.VMEM((rows // 2, 128), F32),
-            pltpu.VMEM((n, rows // 2, 128), BF16),
+            pltpu.VMEM((n, seqs, 128), F32),
+            pltpu.VMEM((3, 2, seqs, 128), F32),
+            pltpu.VMEM((4, 2, seqs, 128), F32),
+            pltpu.VMEM((2, seqs, 128), F32),
+            pltpu.VMEM((seqs, vw), BF16),
+            pltpu.VMEM((2, 2, seqs, vw), BF16),
+            pltpu.VMEM((n, 2, seqs, 512), BF16),
             pltpu.VMEM((msgs, rows // 2, 128), BF16),
             pltpu.VMEM((msgs, rows // 2, 128), BF16),
             pltpu.VMEM((msgs, 2, rows // 4, 128), BF16),
@@ -522,8 +659,8 @@
             pltpu.VMEM((rows // 4, 128), F32),
             pltpu.VMEM((rows // 4, 128), F32),
             dma((20,)),
-            dma((5,)),
-            dma((5,)),
+            dma((6,)),
+            dma((6,)),
             dma((msgs,)),
             dma((msgs,)),
             dma((msgs,)),
@@ -534,7 +671,8 @@
             dma((msgs,)),
             dma((2 * msgs,)),
             dma((2 * msgs,)),
-            pltpu.SemaphoreType.REGULAR((2,)),
+            dma((7 + columns,)),
+            dma((7 + columns,)),
         ],
         compiler_params=pltpu.CompilerParams(collective_id=0, has_side_effects=True, vmem_limit_bytes=40 * 2**20),
         name="cell_step",
@@ -589,7 +727,7 @@
         P(("kv", "tp"), None),
     )
     return jax.shard_map(
-        functools.partial(shards, mesh.shape["kv"]),
+        functools.partial(shards, mesh.shape["kv"], mesh.shape["dp"]),
         mesh=mesh,
         in_specs=placed,
         out_specs=(

time: 98.7 us -> 103 us (1.044)
  Pallas kernels: 97 us -> 102 us
    pallas_call x1, Pallas kernels: 96 us -> 101 us  [shards(): pl.pallas_call(functools.partial(kernel, n, columns), out_shape=(pltpu.VM...]
where the time goes in v4:
time: 103 us
  Pallas kernels  102 us (99%)
    pallas_call x1, Pallas kernels, shards(): pl.pallas_call(functools.partial(kernel, n, columns), out_shape=(pltpu.VM...  101 us

profile of v4, /device:TPU:65, one launch (start us, length us, event | category | flops | bytes accessed | tf_op | source)
XLA Modules:
  0.0 102.9 jit_solution(6251182871443034496)
XLA Ops:
  0.6 101.2 %cell_step.1 = (bf16[64,128]{1,0:T(8,128)(2,1)S(1)}, f32[8,4,64,128]{3,2,1,0:T(8,128)S(1)}, f32[8,256]{1,0:T(8,128)S(1)}, f32[4,8]{1,0:T(4,128)S(1)}) custom-call(bf16[64,128]{1,0:T(8,128)(2,1)} %bitcast.10, f32[1,128]{1,0:T(1,128)} %bitcast.15, bf16[128,256]{1,0:T(8,128)(2,1)} %wq.1, bf16[128,256]{1,0:T(8,128)(2,1)} %wk.1, bf16[128,512]{1,0:T(8,128)(2,1)} %wv.1, ...), custom_call_target="tpu_custom_call" | custom-call | tf_op jit(solution)/shard_map/cell_step/pallas_call | solution.py:619
  101.8 1.0 hand_over.1

commit v5 on v4

--- a/solution.py
+++ b/solution.py
@@ -144,6 +144,7 @@
         loads[name] = c
 
     load("tok", tok, tokb.at[tp])
+    load("wo", wo, wob.at[tp, :, 0:128])
     load("ngain", ngain, ngv)
     load("wq", wq, wp.at[:, 0:hw])
     load("wk", wk, wp.at[:, hw : 2 * hw])
@@ -156,7 +157,6 @@
     load("stab", stab, stabb)
     load("nrm", nrm, nrmb)
     load("mem", mem, memb)
-    load("wo", wo, wob.at[tp, :, 0:128])
     load("mgain", mgain, mgb)
     load("wup", wup, wupb.at[tp])
     load("wdn", wdn, wdnb.at[tp])
@@ -172,6 +172,83 @@
     tok_x = to_partner(tokb.at[tp], tokb.at[tp], 0)
     tok_x.start()
     sends = [tok_x]
+
+    stride = n // 4
+    piece_rows = wo_rows // columns
+    parity = lax.rem(me, 2)
+    mine_offset = jnp.where(tp == parity, 0, -1)
+
+    def piece(x):
+        return pl.ds(pl.multiple_of(x * piece_rows, piece_rows), piece_rows)
+
+    def lanes(slot):
+        return pl.ds(slot * 128, 128)
+
+    def hop(src, dst, i, step, side="kv"):
+        where = at(me + step) if side == "kv" else lax.rem(column + step, columns)
+        return pltpu.make_async_remote_copy(
+            src_ref=src, dst_ref=dst, send_sem=pre_s.at[i], recv_sem=pre_r.at[i], device_id={side: where}, device_id_type=MESH
+        )
+
+    def piece_hop(source, slot, i, step):
+        return hop(wob.at[tp, piece(column), lanes(source)], wob.at[tp, piece(column), lanes(slot)], i, step)
+
+    pre = {
+        "w_up": piece_hop(0, 3, 0, stride),
+        "w_dn": piece_hop(0, 1, 1, -stride),
+        "t_up": hop(tst.at[0], tokx.at[3], 2, stride),
+        "t_dn": hop(tst.at[1], tokx.at[1], 3, -stride),
+        "t_on": hop(tst.at[2], tfwd, 4, stride),
+        "w_fw": piece_hop(3, 2, 5, stride),
+        "t_fw": hop(tfwd, tokx.at[2], 6, stride),
+    }
+
+    def begin(c):
+        c.start()
+        sends.append(c)
+
+    def column_copy(slot, step):
+        part = wob.at[tp, piece(column), lanes(slot)]
+        return hop(part, part, 7 + (slot - 1) * (columns - 1) + step - 1, step, "dp")
+
+    def column_arrival(slot, step):
+        part = wob.at[tp, piece(lax.rem(column - step + columns, columns)), lanes(slot)]
+        return hop(part, part, 7 + (slot - 1) * (columns - 1) + step - 1, step, "dp")
+
+    by_distance = sorted(range(1, columns), key=lambda step: -min(step, columns - step))
+
+    def to_columns(slot):
+        for step in by_distance:
+            begin(column_copy(slot, step))
+
+    def from_columns(slot):
+        for step in range(1, columns):
+            column_arrival(slot, step).wait_recv()
+
+    def share_slot(slot):
+        part = wob.at[tp, :, lanes(slot)]
+        return to_partner(part, part, 6 + slot)
+
+    def forward_on():
+        pre["w_up"].wait_recv()
+        begin(pre["w_fw"])
+        to_columns(3)
+        pre["t_on"].wait_recv()
+        begin(pre["t_fw"])
+        pre["w_dn"].wait_recv()
+        to_columns(1)
+
+    def complete_near():
+        pre["w_fw"].wait_recv()
+        to_columns(2)
+        for slot in (3, 1):
+            from_columns(slot)
+            begin(share_slot(slot))
+
+    loads["wo"].wait()
+    begin(pre["w_up"])
+    begin(pre["w_dn"])
+    begin(share_slot(0))
 
     for name in ("ngain", "wq", "wk", "wv", "wg", "wi", "wf"):
         loads[name].wait()
@@ -274,67 +351,9 @@
 
         return finish
 
-    stride = n // 4
-    piece = pl.ds(pl.multiple_of(column * (wo_rows // columns), wo_rows // columns), wo_rows // columns)
-    parity = lax.rem(me, 2)
-    mine_offset = jnp.where(tp == parity, 0, -1)
-
-    def lanes(slot):
-        return pl.ds(slot * 128, 128)
-
-    def hop(src, dst, i, step, side="kv"):
-        where = at(me + step) if side == "kv" else lax.rem(column + step, columns)
-        return pltpu.make_async_remote_copy(
-            src_ref=src, dst_ref=dst, send_sem=pre_s.at[i], recv_sem=pre_r.at[i], device_id={side: where}, device_id_type=MESH
-        )
-
-    def piece_hop(source, slot, i, step):
-        return hop(wob.at[tp, piece, lanes(source)], wob.at[tp, piece, lanes(slot)], i, step)
-
     for i, step in enumerate((stride, -stride, 2 * stride)):
         for b in range(2):
-            tst[i, b] = tokrow[at(me + step + mine_offset + 2 * b)]
-    loads["wo"].wait()
-    pre = {
-        "w_up": piece_hop(0, 3, 0, stride),
-        "w_dn": piece_hop(0, 1, 1, -stride),
-        "t_up": hop(tst.at[0], tokx.at[3], 2, stride),
-        "t_dn": hop(tst.at[1], tokx.at[1], 3, -stride),
-        "t_on": hop(tst.at[2], tfwd, 4, stride),
-        "w_fw": piece_hop(3, 2, 5, stride),
-        "t_fw": hop(tfwd, tokx.at[2], 6, stride),
-    }
-
-    def begin(c):
-        c.start()
-        sends.append(c)
-
-    for name in ("w_up", "w_dn", "t_up", "t_dn", "t_on"):
-        begin(pre[name])
-    wo_x = to_partner(wob.at[tp, :, lanes(0)], wob.at[tp, :, lanes(0)], 3)
-    begin(wo_x)
-
-    def forward_on():
-        pre["w_up"].wait_recv()
-        pre["t_on"].wait_recv()
-        begin(pre["w_fw"])
-        begin(pre["t_fw"])
-
-    def to_columns():
-        pre["w_dn"].wait_recv()
-        pre["w_fw"].wait_recv()
-        for step in range(1, columns):
-            begin(column_copy(step))
-
-    def column_copy(step):
-        part = wob.at[tp, piece, 128:512]
-        return hop(part, part, 7 + step, step, "dp")
-
-    def column_arrival(step):
-        rows_there = wo_rows // columns
-        theirs = pl.ds(pl.multiple_of(lax.rem(column - step + columns, columns) * rows_there, rows_there), rows_there)
-        part = wob.at[tp, theirs, 128:512]
-        return hop(part, part, 7 + step, step, "dp")
+            tst[i, b] = tokrow[at(me + step + mine_offset + 2 * b)].astype(BF16)
 
     def own_proj(d):
         return pf[d, :, 0:proj], pf[d, :, proj:]
@@ -356,8 +375,10 @@
         i = m[0]
         return [along(m, ps.at[i], pr.at[i], ps_s.at[i], ps_r.at[i])]
 
+    for name in ("t_on", "t_up", "t_dn"):
+        begin(pre[name])
     last = reduce_scatter(PROJ_TREE, own_proj, emit_proj, proj_copies, forward_on)
-    to_columns()
+    complete_near()
 
     loads["wup"].wait()
     loads["wdn"].wait()
@@ -458,12 +479,8 @@
             col = kt[h * qk : (h + 1) * qk, s : s + 1]
             mem_new[s, h] = keep[s : s + 1, h : h + 1] * memb[s, h] + col * v[s : s + 1, h * vd : (h + 1) * vd]
 
-    for step in range(1, columns):
-        column_arrival(step).wait_recv()
-    far = wob.at[tp, :, 128:512]
-    far_x = to_partner(far, far, 4)
-    begin(far_x)
-    wo_x.wait_recv()
+    from_columns(2)
+    begin(share_slot(2))
     for name in ("t_up", "t_dn", "t_fw"):
         pre[name].wait_recv()
 
@@ -478,8 +495,7 @@
         ).wait_recv()
 
     for i in range(2):
-        tokx[0, i] = tokrow[at(me + mine_offset + 2 * i)]
-    far_x.wait_recv()
+        tokx[0, i] = tokrow[at(me + mine_offset + 2 * i)].astype(BF16)
 
     @pl.when(tp != parity)
     def _():
@@ -489,6 +505,8 @@
     hid_arrival(0, other)
     for core in range(2):
         hid_arrival(1, core)
+    for slot in range(4):
+        share_slot(slot).wait_recv()
     left_rows = jnp.concatenate(
         [jnp.concatenate([hidg[i, h].astype(F32) for h in range(2)], axis=1) for i in range(2)], axis=0
     ).astype(BF16)
@@ -497,7 +515,7 @@
     )
     for slot in range(4):
         cols = lax.rem(me // 4 + slot, 4)
-        block = added[:, slot * 128 : (slot + 1) * 128].reshape(2, seqs, 128) + tokx[slot]
+        block = added[:, slot * 128 : (slot + 1) * 128].reshape(2, seqs, 128) + tokx[slot].astype(F32)
         midg[me, :, :, pl.ds(pl.multiple_of(cols * 128, 128), 128)] = block.astype(BF16)
     all_gather(MID_TREE, midg, mid_s, mid_r)()
 
@@ -646,9 +664,9 @@
             pltpu.VMEM((seqs, proj), F32),
             pltpu.VMEM((seqs, vw), F32),
             pltpu.VMEM((n, seqs, 128), F32),
-            pltpu.VMEM((3, 2, seqs, 128), F32),
-            pltpu.VMEM((4, 2, seqs, 128), F32),
-            pltpu.VMEM((2, seqs, 128), F32),
+            pltpu.VMEM((3, 2, seqs, 128), BF16),
+            pltpu.VMEM((4, 2, seqs, 128), BF16),
+            pltpu.VMEM((2, seqs, 128), BF16),
             pltpu.VMEM((seqs, vw), BF16),
             pltpu.VMEM((2, 2, seqs, vw), BF16),
             pltpu.VMEM((n, 2, seqs, 512), BF16),
@@ -659,8 +677,8 @@
             pltpu.VMEM((rows // 4, 128), F32),
             pltpu.VMEM((rows // 4, 128), F32),
             dma((20,)),
-            dma((6,)),
-            dma((6,)),
+            dma((10,)),
+            dma((10,)),
             dma((msgs,)),
             dma((msgs,)),
             dma((msgs,)),
@@ -671,8 +689,8 @@
             dma((msgs,)),
             dma((2 * msgs,)),
             dma((2 * msgs,)),
-            dma((7 + columns,)),
-            dma((7 + columns,)),
+            dma((7 + 3 * (columns - 1),)),
+            dma((7 + 3 * (columns - 1),)),
         ],
         compiler_params=pltpu.CompilerParams(collective_id=0, has_side_effects=True, vmem_limit_bytes=40 * 2**20),
         name="cell_step",

time: 103 us -> 96.3 us (0.935)
  Pallas kernels: 102 us -> 95.5 us
    pallas_call x1, Pallas kernels: 101 us -> 94.5 us  [shards(): pl.pallas_call(functools.partial(kernel, n, columns), out_shape=(pltpu.VM...]
where the time goes in v5:
time: 96.3 us; the launch traced here: 96.1 us
  Pallas kernels  95.5 us (99%)
    pallas_call x1, Pallas kernels, shards(): pl.pallas_call(functools.partial(kernel, n, columns), out_shape=(pltpu.VM...  94.5 us

profile of v5, /device:TPU:65, one launch (start us, length us, event | category | flops | bytes accessed | tf_op | source)
XLA Modules:
  0.0 96.1 jit_solution(6066340035893503463)
XLA Ops:
  0.6 94.5 %cell_step.1 = (bf16[64,128]{1,0:T(8,128)(2,1)S(1)}, f32[8,4,64,128]{3,2,1,0:T(8,128)S(1)}, f32[8,256]{1,0:T(8,128)S(1)}, f32[4,8]{1,0:T(4,128)S(1)}) custom-call(bf16[64,128]{1,0:T(8,128)(2,1)} %bitcast.10, f32[1,128]{1,0:T(1,128)} %bitcast.15, bf16[128,256]{1,0:T(8,128)(2,1)} %wq.1, bf16[128,256]{1,0:T(8,128)(2,1)} %wk.1, bf16[128,512]{1,0:T(8,128)(2,1)} %wv.1, ...), custom_call_target="tpu_custom_call" | custom-call | tf_op jit(solution)/shard_map/cell_step/pallas_call | solution.py:637
  95.1 1.0 %hand_over.1 = (bf16[64,128]{1,0:T(8,128)(2,1)}, f32[8,4,64,128]{3,2,1,0:T(8,128)}, f32[8,256]{1,0:T(8,128)}, f32[4,8]{1,0:T(4,128)}) custom-call(bf16[64,128]{1,0:T(8,128)(2,1)S(1)} %get-tuple-element.12.refs_0_, f32[8,4,64,128]{3,2,1,0:T(8,128)S(1)} %get-tuple-element.13.refs_1_, f32[8,256]{1,0:T(8,128)S(1)} %get-tuple-element.14.refs_2_, ...), custom_call_target="tpu_custom_call" | custom-call | tf_op jit(solution)/shard_map/hand_over/pallas_call | solution.py:716

commit v6 on v5

--- a/solution.py
+++ b/solution.py
@@ -20,16 +20,16 @@
 
 
 def messages(tree, n):
-    half = n // 2
     out = []
-    for side, last in ((1, half), (-1, n - 1 - half)):
-        for k in range(1, last + 1):
+    for side in (1, -1):
+        for k in range(1, n // 2):
             out.append((len(out), side, k, tree[k]))
+    out.append((len(out), 0, n // 2, tree[n // 2]))
     return out
 
 
 def children_of(msgs, side, k):
-    return [m for m in msgs if m[1] == side and m[3] == k]
+    return [m for m in msgs if m[1] in (side, 0) and m[3] == k and k > 0]
 
 
 def depth_below(msgs, m):
@@ -128,6 +128,11 @@
     def at(z):
         return lax.rem(z + 2 * n, n)
 
+    far_side = 1 - 2 * lax.rem(me, 2)
+
+    def way(side):
+        return far_side if side == 0 else side
+
     barrier = pltpu.get_barrier_semaphore()
     for step in range(1, REACH + 1):
         for side in (1, -1):
@@ -182,7 +187,7 @@
         return pl.ds(pl.multiple_of(x * piece_rows, piece_rows), piece_rows)
 
     def lanes(slot):
-        return pl.ds(slot * 128, 128)
+        return pl.ds(slot * 128 if isinstance(slot, int) else pl.multiple_of(slot * 128, 128), 128)
 
     def hop(src, dst, i, step, side="kv"):
         where = at(me + step) if side == "kv" else lax.rem(column + step, columns)
@@ -198,9 +203,9 @@
         "w_dn": piece_hop(0, 1, 1, -stride),
         "t_up": hop(tst.at[0], tokx.at[3], 2, stride),
         "t_dn": hop(tst.at[1], tokx.at[1], 3, -stride),
-        "t_on": hop(tst.at[2], tfwd, 4, stride),
-        "w_fw": piece_hop(3, 2, 5, stride),
-        "t_fw": hop(tfwd, tokx.at[2], 6, stride),
+        "t_on": hop(tst.at[2], tfwd, 4, far_side * stride),
+        "w_fw": piece_hop(2 + far_side, 2, 5, far_side * stride),
+        "t_fw": hop(tfwd, tokx.at[2], 6, far_side * stride),
     }
 
     def begin(c):
@@ -231,12 +236,12 @@
 
     def forward_on():
         pre["w_up"].wait_recv()
+        pre["w_dn"].wait_recv()
         begin(pre["w_fw"])
         to_columns(3)
+        to_columns(1)
         pre["t_on"].wait_recv()
         begin(pre["t_fw"])
-        pre["w_dn"].wait_recv()
-        to_columns(1)
 
     def complete_near():
         pre["w_fw"].wait_recv()
@@ -277,16 +282,19 @@
     def reduce_scatter(tree, own, emit, copies_of, before_relays=None):
         msgs = messages(tree, n)
         order = sorted(msgs, key=lambda m: (depth_below(msgs, m), -level_of(tree, m[2]), -m[2]))
+        waited = set()
         for m in order:
             slot, side, k, parent = m
-            mine = own(at(me - side * k))
+            mine = own(at(me - way(side) * k))
             kids = children_of(msgs, side, k)
             if kids and before_relays is not None:
                 before_relays()
                 before_relays = None
             for c in kids:
-                copies_of(c)[0].wait_recv()
-            emit(m, mine, [c[0] for c in kids])
+                if c[0] not in waited:
+                    waited.add(c[0])
+                    copies_of(c)[0].wait_recv()
+            emit(m, mine, [(c[0], None if c[1] else far_side == side) for c in kids])
             for c in copies_of(m):
                 c.start()
                 sends.append(c)
@@ -294,7 +302,7 @@
 
     def along(m, src, dst, send_sem, recv_sem, core=None):
         slot, side, k, parent = m
-        where = {"kv": at(me - side * (k - parent))}
+        where = {"kv": at(me - way(side) * (k - parent))}
         if core is not None:
             where["tp"] = core
         return pltpu.make_async_remote_copy(
@@ -306,6 +314,7 @@
 
         def copy_of(m):
             slot, side, k, parent = m
+            side = way(side)
             origin = at(me - side * parent)
             return pltpu.make_async_remote_copy(
                 src_ref=buf.at[origin],
@@ -318,6 +327,7 @@
 
         def arrival(m):
             slot, side, k, parent = m
+            side = way(side)
             origin = at(me - side * k)
             return pltpu.make_async_remote_copy(
                 src_ref=buf.at[origin],
@@ -343,8 +353,8 @@
             for m in todo:
                 arrival(m).wait_recv()
                 waited.add(m[0])
-                for c in sorted(children_of(msgs, m[1], m[2]), key=lambda c: (-depth_below(msgs, c), -c[2])):
-                    send(c)
+            for c in sorted([c for c in msgs if c[3]], key=lambda c: (level_of(tree, c[2]), -c[2])):
+                send(c)
             for m in msgs:
                 if m[0] not in waited:
                     arrival(m).wait_recv()
@@ -360,9 +370,12 @@
 
     def sum_proj(mine, slots):
         a, g = mine
-        for s in slots:
-            a = a + pr[s, :, 0:proj].astype(F32)
-            g = g + pr[s, :, proj:].astype(F32)
+        for s, here in slots:
+            more_a, more_g = pr[s, :, 0:proj].astype(F32), pr[s, :, proj:].astype(F32)
+            if here is not None:
+                more_a, more_g = jnp.where(here, more_a, 0.0), jnp.where(here, more_g, 0.0)
+            a = a + more_a
+            g = g + more_g
         return a, g
 
     def emit_proj(m, mine, slots):
@@ -392,7 +405,7 @@
 
     for m in last:
         proj_copies(m)[0].wait_recv()
-    slots = [m[0] for m in last]
+    slots = [(m[0], None) for m in last]
     total, gate = sum_proj(own_proj(me), slots)
     sf[:, 0:proj] = total
     squares = gate[:, gate_lanes : gate_lanes + 1] + gate[:, gate_lanes + 1 : gate_lanes + 2]
@@ -556,8 +569,9 @@
         )
 
     def sum_down(a, slots):
-        for s in slots:
-            a = a + dr[s].astype(F32)
+        for s, here in slots:
+            more = dr[s].astype(F32)
+            a = a + (more if here is None else jnp.where(here, more, 0.0))
         return a
 
     def halves(a):
@@ -594,6 +608,10 @@
     fin_x = to_partner(fxs, fxr, 5)
     fin_x.start()
     sends.append(fin_x)
+    early = len(sends)
+    for c in sends[:-1]:
+        c.wait_send()
+    early -= 1
     fin_x.wait_recv()
     sums = [jnp.where(tp == 0, left, right), fxr[...]]
     sums = [jnp.where(tp == 0, sums[0], sums[1]), jnp.where(tp == 0, sums[1], sums[0])]
@@ -606,7 +624,7 @@
         [sums[r][m * seqs : (m + 1) * seqs] for m in range(blocks // 2) for r in range(2)], axis=0
     ).T
     out[...] = jnp.concatenate([flat[0:half_ch], flat[half_ch : 2 * half_ch]], axis=1).astype(BF16)
-    for c in sends:
+    for c in sends[early:]:
         c.wait_send()
 
 

time: 96.3 us -> 95.3 us (0.990)
  Pallas kernels: 95.5 us -> 94.5 us
    pallas_call x1, Pallas kernels: 94.5 us -> 93.5 us  [shards(): pl.pallas_call(functools.partial(kernel, n, columns), out_shape=(pltpu.VM...]
where the time goes in v6:
time: 95.3 us; the launch traced here: 95.1 us
  Pallas kernels  94.5 us (99%)
    pallas_call x1, Pallas kernels, shards(): pl.pallas_call(functools.partial(kernel, n, columns), out_shape=(pltpu.VM...  93.5 us

profile of v6, /device:TPU:65, one launch (start us, length us, event | category | flops | bytes accessed | tf_op | source)
XLA Modules:
  0.0 95.1 jit_solution(5994979064279950927)
XLA Ops:
  0.6 93.5 %cell_step.1 = (bf16[64,128]{1,0:T(8,128)(2,1)S(1)}, f32[8,4,64,128]{3,2,1,0:T(8,128)S(1)}, f32[8,256]{1,0:T(8,128)S(1)}, f32[4,8]{1,0:T(4,128)S(1)}) custom-call(bf16[64,128]{1,0:T(8,128)(2,1)} %bitcast.10, f32[1,128]{1,0:T(1,128)} %bitcast.15, bf16[128,256]{1,0:T(8,128)(2,1)} %wq.1, bf16[128,256]{1,0:T(8,128)(2,1)} %wk.1, bf16[128,512]{1,0:T(8,128)(2,1)} %wv.1, ...), custom_call_target="tpu_custom_call" | custom-call | tf_op jit(solution)/shard_map/cell_step/pallas_call | solution.py:655
  94.1 1.0 %hand_over.1 = (bf16[64,128]{1,0:T(8,128)(2,1)}, f32[8,4,64,128]{3,2,1,0:T(8,128)}, f32[8,256]{1,0:T(8,128)}, f32[4,8]{1,0:T(4,128)}) custom-call(bf16[64,128]{1,0:T(8,128)(2,1)S(1)} %get-tuple-element.12.refs_0_, f32[8,4,64,128]{3,2,1,0:T(8,128)S(1)} %get-tuple-element.13.refs_1_, f32[8,256]{1,0:T(8,128)S(1)} %get-tuple-element.14.refs_2_, ...), custom_call_target="tpu_custom_call" | custom-call | tf_op jit(solution)/shard_map/hand_over/pallas_call | solution.py:734

commit v7 on v6

--- a/solution.py
+++ b/solution.py
@@ -13,7 +13,7 @@
 BF16 = jnp.bfloat16
 
 TWO_LEVEL = {1: 0, 2: 0, 3: 0, 4: 0, 5: 4, 6: 4, 7: 4, 8: 4}
-PROJ_TREE = TWO_LEVEL
+PROJ_TREE = {1: 0, 2: 0, 3: 0, 4: 3, 5: 3, 6: 3, 7: 6, 8: 6}
 REACH = 4
 MID_TREE = TWO_LEVEL
 DOWN_TREE = TWO_LEVEL
@@ -234,21 +234,25 @@
         part = wob.at[tp, :, lanes(slot)]
         return to_partner(part, part, 6 + slot)
 
+    up_x = to_partner(wupb.at[tp], wupb.at[tp], 1)
+    dn_x = to_partner(wdnb.at[tp], wdnb.at[tp], 2)
+
     def forward_on():
+        loads["wup"].wait()
+        begin(up_x)
+        loads["wdn"].wait()
+        begin(dn_x)
         pre["w_up"].wait_recv()
         pre["w_dn"].wait_recv()
         begin(pre["w_fw"])
         to_columns(3)
         to_columns(1)
+
+    def complete_near():
         pre["t_on"].wait_recv()
         begin(pre["t_fw"])
-
-    def complete_near():
         pre["w_fw"].wait_recv()
         to_columns(2)
-        for slot in (3, 1):
-            from_columns(slot)
-            begin(share_slot(slot))
 
     loads["wo"].wait()
     begin(pre["w_up"])
@@ -393,13 +397,6 @@
     last = reduce_scatter(PROJ_TREE, own_proj, emit_proj, proj_copies, forward_on)
     complete_near()
 
-    loads["wup"].wait()
-    loads["wdn"].wait()
-    up_x = to_partner(wupb.at[tp], wupb.at[tp], 1)
-    up_x.start()
-    dn_x = to_partner(wdnb.at[tp], wdnb.at[tp], 2)
-    dn_x.start()
-    sends += [up_x, dn_x]
     for name in ("ib", "fb", "stab", "nrm", "mem", "mgain"):
         loads[name].wait()
 
@@ -486,12 +483,9 @@
     def _():
         hidg[0, tp] = hid_own[...]
 
-    kt = tk.T
-    for s in range(seqs):
-        for h in range(heads):
-            col = kt[h * qk : (h + 1) * qk, s : s + 1]
-            mem_new[s, h] = keep[s : s + 1, h : h + 1] * memb[s, h] + col * v[s : s + 1, h * vd : (h + 1) * vd]
-
+    for slot in (3, 1):
+        from_columns(slot)
+        begin(share_slot(slot))
     from_columns(2)
     begin(share_slot(2))
     for name in ("t_up", "t_dn", "t_fw"):
@@ -530,7 +524,15 @@
         cols = lax.rem(me // 4 + slot, 4)
         block = added[:, slot * 128 : (slot + 1) * 128].reshape(2, seqs, 128) + tokx[slot].astype(F32)
         midg[me, :, :, pl.ds(pl.multiple_of(cols * 128, 128), 128)] = block.astype(BF16)
-    all_gather(MID_TREE, midg, mid_s, mid_r)()
+    finish = all_gather(MID_TREE, midg, mid_s, mid_r)
+
+    kt = tk.T
+    for s in range(seqs):
+        for h in range(heads):
+            col = kt[h * qk : (h + 1) * qk, s : s + 1]
+            mem_new[s, h] = keep[s : s + 1, h : h + 1] * memb[s, h] + col * v[s : s + 1, h * vd : (h + 1) * vd]
+
+    finish()
 
     up_x.wait_recv()
     dn_x.wait_recv()

time: 95.3 us -> 94.6 us (level)
  no operation moved by 1% of the time
where the time goes in v7:
time: 94.6 us; the launch traced here: 94.4 us
  Pallas kernels  93.7 us (99%)
    pallas_call x1, Pallas kernels, shards(): pl.pallas_call(functools.partial(kernel, n, columns), out_shape=(pltpu.VM...  92.7 us

profile of v7, /device:TPU:65, one launch (start us, length us, event | category | flops | bytes accessed | tf_op | source)
XLA Modules:
  0.0 94.4 jit_solution(18406533399915885314)
XLA Ops:
  0.6 92.7 %cell_step.1 = (bf16[64,128]{1,0:T(8,128)(2,1)S(1)}, f32[8,4,64,128]{3,2,1,0:T(8,128)S(1)}, f32[8,256]{1,0:T(8,128)S(1)}, f32[4,8]{1,0:T(4,128)S(1)}) custom-call(bf16[64,128]{1,0:T(8,128)(2,1)} %bitcast.10, f32[1,128]{1,0:T(1,128)} %bitcast.15, bf16[128,256]{1,0:T(8,128)(2,1)} %wq.1, bf16[128,256]{1,0:T(8,128)(2,1)} %wk.1, bf16[128,512]{1,0:T(8,128)(2,1)} %wv.1, ...), custom_call_target="tpu_custom_call" | custom-call | tf_op jit(solution)/shard_map/cell_step/pallas_call | solution.py:657
  93.4 1.0 %hand_over.1 = (bf16[64,128]{1,0:T(8,128)(2,1)}, f32[8,4,64,128]{3,2,1,0:T(8,128)}, f32[8,256]{1,0:T(8,128)}, f32[4,8]{1,0:T(4,128)}) custom-call(bf16[64,128]{1,0:T(8,128)(2,1)S(1)} %get-tuple-element.12.refs_0_, f32[8,4,64,128]{3,2,1,0:T(8,128)S(1)} %get-tuple-element.13.refs_1_, f32[8,256]{1,0:T(8,128)S(1)} %get-tuple-element.14.refs_2_, ...), custom_call_target="tpu_custom_call" | custom-call | tf_op jit(solution)/shard_map/hand_over/pallas_call | solution.py:736

commit v8 on v7

--- a/solution.py
+++ b/solution.py
@@ -283,7 +283,7 @@
         upper = total.astype(BF16).astype(F32)
         return jnp.where(lane8 == gate_lanes, upper, jnp.where(lane8 == gate_lanes + 1, total - upper, g))
 
-    def reduce_scatter(tree, own, emit, copies_of, before_relays=None):
+    def reduce_scatter(tree, own, add, emit, copies_of, before_relays=None):
         msgs = messages(tree, n)
         order = sorted(msgs, key=lambda m: (depth_below(msgs, m), -level_of(tree, m[2]), -m[2]))
         waited = set()
@@ -298,7 +298,8 @@
                 if c[0] not in waited:
                     waited.add(c[0])
                     copies_of(c)[0].wait_recv()
-            emit(m, mine, [(c[0], None if c[1] else far_side == side) for c in kids])
+                mine = add(mine, [(c[0], None if c[1] else far_side == side)])
+            emit(m, mine)
             for c in copies_of(m):
                 c.start()
                 sends.append(c)
@@ -382,9 +383,9 @@
             g = g + more_g
         return a, g
 
-    def emit_proj(m, mine, slots):
+    def emit_proj(m, mine):
         slot = m[0]
-        a, g = sum_proj(mine, slots)
+        a, g = mine
         ps[slot, :, 0:proj] = a.astype(BF16)
         ps[slot, :, proj:] = pack_gates(g).astype(BF16)
 
@@ -394,16 +395,16 @@
 
     for name in ("t_on", "t_up", "t_dn"):
         begin(pre[name])
-    last = reduce_scatter(PROJ_TREE, own_proj, emit_proj, proj_copies, forward_on)
+    last = reduce_scatter(PROJ_TREE, own_proj, sum_proj, emit_proj, proj_copies, forward_on)
     complete_near()
 
     for name in ("ib", "fb", "stab", "nrm", "mem", "mgain"):
         loads[name].wait()
 
-    for m in last:
+    total, gate = own_proj(me)
+    for m in sorted(last, key=lambda m: m[2]):
         proj_copies(m)[0].wait_recv()
-    slots = [(m[0], None) for m in last]
-    total, gate = sum_proj(own_proj(me), slots)
+        total, gate = sum_proj((total, gate), [(m[0], None)])
     sf[:, 0:proj] = total
     squares = gate[:, gate_lanes : gate_lanes + 1] + gate[:, gate_lanes + 1 : gate_lanes + 2]
     rscale = lax.rsqrt(squares / width + EPSILON)
@@ -585,8 +586,7 @@
     quarter = half_rows // 2
     msgs_n = n - 1
 
-    def emit_down(m, mine, slots):
-        a = sum_down(mine, slots)
+    def emit_down(m, a):
         if m[3] == 0:
             fs[m[0], 0], fs[m[0], 1] = [x.astype(BF16) for x in halves(a)]
         else:
@@ -600,7 +600,7 @@
             ]
         return [along(m, ds.at[i], dr.at[i], dn_s.at[i], dn_r.at[i])]
 
-    last = reduce_scatter(DOWN_TREE, own_down, emit_down, down_copies)
+    last = reduce_scatter(DOWN_TREE, own_down, sum_down, emit_down, down_copies)
     own_mid = []
     for m in range(blocks):
         z, half = place(lax.rem(me, 4), m)

time: 94.6 us -> 94.6 us (level)
  no operation moved by 1% of the time
where the time goes in v8:
time: 94.6 us; the launch traced here: 94.4 us
  Pallas kernels  93.8 us (99%)
    pallas_call x1, Pallas kernels, shards(): pl.pallas_call(functools.partial(kernel, n, columns), out_shape=(pltpu.VM...  92.7 us

profile of v8, /device:TPU:65, one launch (start us, length us, event | category | flops | bytes accessed | tf_op | source)
XLA Modules:
  0.0 94.4 jit_solution(15778367551815958794)
XLA Ops:
  0.6 92.7 %cell_step.1 = (bf16[64,128]{1,0:T(8,128)(2,1)S(1)}, f32[8,4,64,128]{3,2,1,0:T(8,128)S(1)}, f32[8,256]{1,0:T(8,128)S(1)}, f32[4,8]{1,0:T(4,128)S(1)}) custom-call(bf16[64,128]{1,0:T(8,128)(2,1)} %bitcast.10, f32[1,128]{1,0:T(1,128)} %bitcast.15, bf16[128,256]{1,0:T(8,128)(2,1)} %wq.1, bf16[128,256]{1,0:T(8,128)(2,1)} %wk.1, bf16[128,512]{1,0:T(8,128)(2,1)} %wv.1, ...), custom_call_target="tpu_custom_call" | custom-call | tf_op jit(solution)/shard_map/cell_step/pallas_call | solution.py:657
  93.4 1.0 %hand_over.1 = (bf16[64,128]{1,0:T(8,128)(2,1)}, f32[8,4,64,128]{3,2,1,0:T(8,128)}, f32[8,256]{1,0:T(8,128)}, f32[4,8]{1,0:T(4,128)}) custom-call(bf16[64,128]{1,0:T(8,128)(2,1)S(1)} %get-tuple-element.12.refs_0_, f32[8,4,64,128]{3,2,1,0:T(8,128)S(1)} %get-tuple-element.13.refs_1_, f32[8,256]{1,0:T(8,128)S(1)} %get-tuple-element.14.refs_2_, ...), custom_call_target="tpu_custom_call" | custom-call | tf_op jit(solution)/shard_map/hand_over/pallas_call | solution.py:736
